TPU v7x, 256 devices: a whole 4x4x8 slice. The times are simulated.
256 devices in a mesh: sp: 16 (over y, x), tp: 16 (over z, core).
Axes of the slice: x: 4, y: 4, z: 8, core: 2. Of those that a mesh axis runs over, the one named last changes fastest.
Arguments:
- gate_b: bfloat16 [8192, 1024], P('sp', 'tp'), may hold values from -6 to 6
- gate_c: bfloat16 [8192, 1024], P('sp', 'tp'), may hold values from -6 to 6
- values_in: bfloat16 [8192, 1024], P('sp', 'tp'), may hold values from -6 to 6
- conv_w: bfloat16 [3, 1024], P(None, 'tp'), may hold values from -3.5 to 3.5
- documents: int32 [8192], P('sp'), may hold values from 0 to 8, never falling along the last dimension, each value on 1 to 4096 neighbouring positions
- w_out: bfloat16 [1024, 2048], replicated, may hold values from -0.1875 to 0.1875
- resid: bfloat16 [8192, 2048], P(('sp', 'tp')), may hold values from -6 to 6
- norm_gain: bfloat16 [2048], replicated, may hold values from 0.099609375 to 1.8984375
- route_ids: int32 [8192, 2], P(('sp', 'tp')), may hold values from 0 to 15, all different within a row; in each aligned block of 32 rows (0 to 31, 32 to 63, ...) at most 8 rows name the same one
- route_weight: float32 [8192, 2], P(('sp', 'tp')), may hold values from 0.2 to 1
- w_gate: bfloat16 [16, 2048, 7168], P('sp', None, 'tp'), may hold values from -0.125 to 0.125
- w_up: bfloat16 [16, 2048, 7168], P('sp', None, 'tp'), may hold values from -0.125 to 0.125
- w_down: bfloat16 [16, 7168, 2048], P('sp', 'tp'), may hold values from -0.0625 to 0.0625
Outputs:
- layer_out: bfloat16 [8192, 2048], P(('sp', 'tp'))
Inputs may be any that keep to these rules, and one draw needn't show every extreme that they name: `route_ids`: each token names two different experts; in the rows of one device no expert is named by more than 8 rows, a bound that some block reaches. `documents`: document numbers never fall along the positions; a document has at most 8192 // 2 positions.
All inputs are finite; a program needn't handle non-finite values.
Results may differ from a plain program's by a relative error of at most 0.018.
Values may be sent and summed in bfloat16 or wider, within the bound.
No kernel may reach another device: no remote copies, remote signals or barrier semaphores. Data moves between devices by JAX's collectives and lax.ppermute only.
A program may use at most 128 MiB of HBM per device.

v0:
```python
import jax
import jax.numpy as jnp
from jax import lax
from jax.sharding import PartitionSpec as P


def passed_along(block, axis, distance):
    devices = range(lax.axis_size(axis))
    route = [(i - distance, i) for i in devices if i - distance in devices]
    return lax.ppermute(block, axis, route)


def local(
    gate_b,
    gate_c,
    values_in,
    conv_w,
    documents,
    w_out,
    resid,
    norm_gain,
    route_ids,
    route_weight,
    w_gate,
    w_up,
    w_down,
):
    seq_rows = gate_b.shape[0]
    local_rows = resid.shape[0]
    model_width = resid.shape[1]
    last_rows = jnp.stack([gate_c[seq_rows - 2 :], values_in[seq_rows - 2 :]])
    before, before_docs = passed_along((last_rows, documents[seq_rows - 2 :]), "sp", 1)
    products = jnp.concatenate(
        [
            before[0].astype(jnp.float32) * before[1].astype(jnp.float32),
            gate_c.astype(jnp.float32) * values_in.astype(jnp.float32),
        ],
        axis=0,
    )
    docs_all = jnp.concatenate([before_docs, documents], axis=0)
    kernel_taps = conv_w.astype(jnp.float32)
    near_mask = (docs_all[1:-1] == documents).astype(jnp.float32)[:, None]
    far_mask = (docs_all[:-2] == documents).astype(jnp.float32)[:, None]
    convolved = (
        kernel_taps[2] * products[2:]
        + kernel_taps[1] * products[1:-1] * near_mask
        + kernel_taps[0] * products[:-2] * far_mask
    )
    mixed_rows = (gate_b.astype(jnp.float32) * convolved).astype(jnp.bfloat16)
    token_rows = lax.all_to_all(mixed_rows, "tp", split_axis=0, concat_axis=1, tiled=True)
    projected = jnp.dot(token_rows, w_out, preferred_element_type=jnp.float32)
    hidden_state = (resid.astype(jnp.float32) + projected).astype(jnp.bfloat16)
    state_wide = hidden_state.astype(jnp.float32)
    normed = (
        state_wide
        * lax.rsqrt(jnp.mean(state_wide * state_wide, axis=-1, keepdims=True) + 1e-06)
        * norm_gain.astype(jnp.float32)
    ).astype(jnp.bfloat16)
    experts = lax.axis_size("sp") * w_gate.shape[0]
    capacity = 4 * local_rows // experts
    flat_ids = route_ids.reshape(-1)
    one_hot = (flat_ids[:, None] == jnp.arange(experts, dtype=jnp.int32)[None, :]).astype(jnp.int32)
    rank_in = jnp.sum((jnp.cumsum(one_hot, axis=0) - one_hot) * one_hot, axis=1)
    slot_index = flat_ids * capacity + rank_in
    placement = (
        slot_index[:, None] == jnp.arange(experts * capacity, dtype=jnp.int32)[None, :]
    ).astype(jnp.bfloat16)
    repeated = jnp.repeat(normed, 2, axis=0)
    dispatch = jnp.einsum(
        "js,jd->sd", placement, repeated, preferred_element_type=jnp.float32
    ).astype(jnp.bfloat16)
    dispatch = dispatch.reshape(experts, capacity, model_width)
    gathered_piece = lax.all_gather(
        lax.all_to_all(dispatch, "sp", split_axis=0, concat_axis=0, tiled=True),
        "tp",
        axis=0,
        tiled=True,
    )
    flat_rows = gathered_piece.reshape(-1, model_width)
    gate_part = jnp.dot(flat_rows, w_gate[0], preferred_element_type=jnp.float32)
    up_part = jnp.dot(flat_rows, w_up[0], preferred_element_type=jnp.float32)
    activated = (jax.nn.silu(gate_part) * up_part).astype(jnp.bfloat16)
    partial_value = jnp.dot(activated, w_down[0], preferred_element_type=jnp.float32)
    partial_value = partial_value.reshape(
        gathered_piece.shape[0], gathered_piece.shape[1], model_width
    )
    summed = lax.psum_scatter(
        partial_value.astype(jnp.bfloat16), "tp", scatter_dimension=0, tiled=True
    )
    returned = lax.all_to_all(summed, "sp", split_axis=0, concat_axis=0, tiled=True)
    picked = jnp.take(
        returned.reshape(experts * capacity, model_width), slot_index, axis=0
    ).reshape(local_rows, 2, model_width)
    combined = jnp.sum(route_weight[:, :, None] * picked.astype(jnp.float32), axis=1)
    return (hidden_state.astype(jnp.float32) + combined).astype(jnp.bfloat16)


def solution(mesh):
    return jax.shard_map(
        local,
        mesh=mesh,
        in_specs=(
            P("sp", "tp"),
            P("sp", "tp"),
            P("sp", "tp"),
            P(None, "tp"),
            P("sp"),
            P(),
            P(("sp", "tp"), None),
            P(),
            P(("sp", "tp"), None),
            P(("sp", "tp"), None),
            P("sp", None, "tp"),
            P("sp", None, "tp"),
            P("sp", "tp", None),
        ),
        out_specs=P(("sp", "tp"), None),
        check_vma=False,
    )
```

profile of v0, /device:TPU:2, one launch (start us, length us, event | category | flops | bytes accessed | tf_op | source)
XLA Modules:
  0.0 234.4 jit_solution(8225996941570353827)
XLA Ops:
  6.5 0.9 slice.43
  7.4 3.4 %collective-permute-start.1 = (s32[2]{0:T(128)S(1)}, s32[2]{0:T(128)S(1)}, u32[]{:S(2)}, u32[]{:S(2)}) collective-permute-start(s32[2]{0:T(128)S(1)} %slice.43), channel_id=1, source_target_pairs={{0,16},{16,32},{32,48},{48,64},{64,80},{80,96},{96,112},{112,128},... | collective-permute-start | bytes 32 | tf_op jit(solution)/shard_map/ppermute | solution.py:10
  10.8 0.8 slice.38
  11.7 0.8 slice.39
  12.6 3.1 %collective-permute-start = (bf16[2,2,64]{2,1,0:T(2,128)(2,1)S(1)}, bf16[2,2,64]{2,1,0:T(2,128)(2,1)S(1)}, u32[]{:S(2)}, u32[]{:S(2)}) collective-permute-start(bf16[2,2,64]{2,1,0:T(2,128)(2,1)S(1)} %pad_maximum_fusion.1), channel_id=1, source_target_pairs={{0,16},{16,32},{32,48},{48,64},{64,80},{80,96},{96,112},{112,128},... | collective-permute-start | bytes 1544 | tf_op jit(solution)/shard_map/ppermute | solution.py:10
  15.7 0.9 convert_multiply_fusion
  16.6 0.7 convert_element_type.66
  17.3 0.7 convert_element_type.77
  18.0 0.8 copy.51
  19.2 0.8 pad_add_fusion
  20.0 0.8 fusion.24
  20.9 1.0 fusion.19
  22.0 0.8 reshape.97
  22.8 8.6 %all-to-all-start = ((bf16[16,2,1024]{2,1,0:T(2,128)(2,1)}), bf16[16,2,1024]{2,1,0:T(2,128)(2,1)S(1)}, u32[]{:S(2)}, u32[]{:S(2)}) async-start(bf16[16,2,1024]{2,1,0:T(2,128)(2,1)} %reshape.97), calls=%async_computation | async-start | bytes 131072 | tf_op jit(solution)/shard_map/all_to_all | solution.py:50
  31.4 7.7 %all-to-all-done = bf16[16,2,1024]{2,1,0:T(2,128)(2,1)S(1)} async-done(((bf16[16,2,1024]{2,1,0:T(2,128)(2,1)}), bf16[16,2,1024]{2,1,0:T(2,128)(2,1)S(1)}, u32[]{:S(2)}, u32[]{:S(2)}) %all-to-all-start) | async-done | bytes 65568 | tf_op jit(solution)/shard_map/all_to_all | solution.py:50
  39.5 3.1 %multiply_reduce_fusion.1 = (f32[32]{0:T(128)S(1)}, f32[32,2048]{1,0:T(8,128)S(1)}) fusion(bf16[32,1024]{1,0:T(8,128)(2,1)S(1)} %all_to_all.23, bf16[1024,2048]{1,0:T(8,128)(2,1)} %param.18, bf16[32,2048]{1,0:T(8,128)(2,1)} %param.19), kind=kOutput, calls=%fused_computation.20 | convolution fusion | flops 134610912 | bytes 4653184 | tf_op jit(solution)/shard_map/dot_general | solution.py:51
  43.0 0.4 fusion.6
  43.4 17.8 %all_to_all.29 = bf16[16,8,2048]{2,1,0:T(8,128)(2,1)} all-to-all(bf16[16,8,2048]{2,1,0:T(8,128)(2,1)S(1)} %fusion.6), channel_id=1, replica_groups=mesh['sp'=16,'tp'=16] {'sp'}, dimensions={0} | all-to-all | bytes 1048576 | tf_op jit(solution)/shard_map/all_to_all | solution.py:74
  61.3 49.6 %all-gather.2.cloned.1.call-done = bf16[256,8,2048]{2,1,0:T(8,128)(2,1)} async-done(((bf16[16,8,2048]{2,1,0:T(8,128)(2,1)}), bf16[256,8,2048]{2,1,0:T(8,128)(2,1)}) %all-gather.2.cloned.1.call-update) | async-done | bytes 8388624 | tf_op jit(solution)/shard_map/all_gather | solution.py:73
  111.0 7.2 %fusion.2 = f32[2048,448]{0,1:T(8,128)S(1)} fusion(bf16[256,8,2048]{2,1,0:T(8,128)(2,1)} %all-gather.2.cloned.1.call-done, bf16[1,2048,448]{1,2,0:T(8,128)(2,1)} %param.23), kind=kOutput, calls=%fused_computation.3 | convolution fusion | flops 3758096384 | bytes 13893632 | tf_op jit(solution)/shard_map/dot_general | solution.py:80
  118.2 5.5 %multiply_convert_fusion = bf16[2048,448]{0,1:T(8,128)(2,1)} fusion(f32[2048,448]{0,1:T(8,128)S(1)} %fusion.2, bf16[256,8,2048]{2,1,0:T(8,128)(2,1)S(1)} %copy-done.3, bf16[1,2048,448]{1,2,0:T(8,128)(2,1)S(1)} %copy-done.4), kind=kOutput, calls=%fused_computation.6 | convolution fusion | flops 3763601408 | bytes 15728640 | tf_op jit(solution)/shard_map/dot_general | solution.py:81
  123.7 3.8 %copy.54 = bf16[2048,448]{1,0:T(8,128)(2,1)} copy(bf16[2048,448]{0,1:T(8,128)(2,1)} %multiply_convert_fusion) | data formatting | bytes 3670016 | tf_op jit(solution)/shard_map/convert_element_type | solution.py:82
  127.5 9.2 %convolution_convert_fusion = bf16[256,8,2048]{2,0,1:T(8,128)(2,1)} fusion(bf16[256,8,448]{2,1,0:T(8,128)(2,1)} %bitcast.43, bf16[1,448,2048]{2,1,0:T(8,128)(2,1)S(1)} %copy-done), kind=kOutput, calls=%fused_computation.5 | convolution fusion | flops 3762290688 | bytes 12058624 | tf_op jit(solution)/shard_map/dot_general | solution.py:83
  136.8 0.5 copy-done.1
  137.6 68.4 %reduce-scatter.2.cloned.1.call-done = bf16[16,8,2048]{2,0,1:T(8,128)(2,1)} async-done(((bf16[256,8,2048]{2,0,1:T(8,128)(2,1)}), bf16[16,8,2048]{2,0,1:T(8,128)(2,1)}) %reduce-scatter.2.cloned.1.call-update) | async-done | bytes 524304 | tf_op jit(solution)/shard_map/reduce_scatter | solution.py:87
  206.1 2.1 copy.56
  208.2 7.3 %all-to-all-start.2 = ((bf16[16,8,2048]{2,1,0:T(8,128)(2,1)}), bf16[16,8,2048]{2,1,0:T(8,128)(2,1)S(1)}, u32[]{:S(2)}, u32[]{:S(2)}) async-start(bf16[16,8,2048]{2,1,0:T(8,128)(2,1)} %copy.56), calls=%async_computation.3 | async-start | bytes 1048576 | tf_op jit(solution)/shard_map/all_to_all | solution.py:90
  215.7 8.6 %all-to-all-done.2 = bf16[16,8,2048]{2,1,0:T(8,128)(2,1)S(1)} async-done(((bf16[16,8,2048]{2,1,0:T(8,128)(2,1)}), bf16[16,8,2048]{2,1,0:T(8,128)(2,1)S(1)}, u32[]{:S(2)}, u32[]{:S(2)}) %all-to-all-start.2) | async-done | bytes 524320 | tf_op jit(solution)/shard_map/all_to_all | solution.py:90
  224.3 0.7 gather_fusion
  225.0 0.2 gather.7
  225.2 1.7 multiply_reduce_fusion
  226.9 0.7 add_convert_fusion
  (44 shorter events, 2.3 us)
Async XLA Ops:
  6.5 120.9 %copy-start = (bf16[1,448,2048]{2,1,0:T(8,128)(2,1)S(1)}, bf16[1,448,2048]{2,1,0:T(8,128)(2,1)}, u32[]{:S(2)}) copy-start(bf16[1,448,2048]{2,1,0:T(8,128)(2,1)} %param.25) | copy-start | bytes 5505028
  7.4 11.8 %collective-permute-start.1 = (s32[2]{0:T(128)S(1)}, s32[2]{0:T(128)S(1)}, u32[]{:S(2)}, u32[]{:S(2)}) collective-permute-start(s32[2]{0:T(128)S(1)} %slice.43), channel_id=1, source_target_pairs={{0,16},{16,32},{32,48},{48,64},{64,80},{80,96},{96,112},{112,128},... | collective-permute-start | bytes 32 | tf_op jit(solution)/shard_map/ppermute | solution.py:10
  12.6 8.1 %collective-permute-start = (bf16[2,2,64]{2,1,0:T(2,128)(2,1)S(1)}, bf16[2,2,64]{2,1,0:T(2,128)(2,1)S(1)}, u32[]{:S(2)}, u32[]{:S(2)}) collective-permute-start(bf16[2,2,64]{2,1,0:T(2,128)(2,1)S(1)} %pad_maximum_fusion.1), channel_id=1, source_target_pairs={{0,16},{16,32},{32,48},{48,64},{64,80},{80,96},{96,112},{112,128},... | collective-permute-start | bytes 1544 | tf_op jit(solution)/shard_map/ppermute | solution.py:10
  22.8 16.4 %all-to-all-start = ((bf16[16,2,1024]{2,1,0:T(2,128)(2,1)}), bf16[16,2,1024]{2,1,0:T(2,128)(2,1)S(1)}, u32[]{:S(2)}, u32[]{:S(2)}) async-start(bf16[16,2,1024]{2,1,0:T(2,128)(2,1)} %reshape.97), calls=%async_computation | async-start | bytes 131072 | tf_op jit(solution)/shard_map/all_to_all | solution.py:50
  31.3 79.6 %all-gather.2.cloned.1.call-start = ((), (), s32[]{:S(2)}) async-start(), calls=%async_computation.4 | async-start | bytes 8912896 | tf_op jit(solution)/shard_map/all_gather | solution.py:73
  61.3 144.8 %reduce-scatter.2.cloned.1.call-start = ((), (), s32[]{:S(2)}) async-start(), calls=%async_computation.5 | async-start | bytes 8912896 | tf_op jit(solution)/shard_map/reduce_scatter | solution.py:87
  110.9 7.2 %copy-start.3 = (bf16[256,8,2048]{2,1,0:T(8,128)(2,1)S(1)}, bf16[256,8,2048]{2,1,0:T(8,128)(2,1)}, u32[]{:S(2)}) copy-start(bf16[256,8,2048]{2,1,0:T(8,128)(2,1)} %all-gather.2.cloned.1.call-done) | copy-start | bytes 25165828
  111.0 7.2 %copy-start.4 = (bf16[1,2048,448]{1,2,0:T(8,128)(2,1)S(1)}, bf16[1,2048,448]{1,2,0:T(8,128)(2,1)}, u32[]{:S(2)}) copy-start(bf16[1,2048,448]{1,2,0:T(8,128)(2,1)} %param.24) | copy-start | bytes 5505028
  136.7 0.7 copy-start.1
  136.7 78.9 %copy-start.2 = (f32[32,2]{0,1:T(2,128)S(1)}, f32[32,2]{0,1:T(2,128)}, u32[]{:S(2)}) copy-start(f32[32,2]{0,1:T(2,128)} %param.22) | copy-start | bytes 772
  208.2 16.1 %all-to-all-start.2 = ((bf16[16,8,2048]{2,1,0:T(8,128)(2,1)}), bf16[16,8,2048]{2,1,0:T(8,128)(2,1)S(1)}, u32[]{:S(2)}, u32[]{:S(2)}) async-start(bf16[16,8,2048]{2,1,0:T(8,128)(2,1)} %copy.56), calls=%async_computation.3 | async-start | bytes 1048576 | tf_op jit(solution)/shard_map/all_to_all | solution.py:90
Sparse Core Ops, SparseCore 0:
  61.4 49.4 all-gather.1
  136.8 69.2 reduce-scatter.1
where the time goes:
time: 235 us; the launch traced here: 234 us
  waiting for transfers between devices  134 us (57%)
  matrix products  25.4 us (11%)
  starting transfers between devices  22.4 us (10%)
  blocking collectives  17.8 us (8%)
  between operations  13.6 us (6%)
  local copies, waits for them, and re-layouts  13.1 us (6%)
  other arithmetic  7.69 us (3%)
    reduce_scatter x1, waiting for transfers between devices, local(): lax.psum_scatter(partial_value.astype(jnp.bfloat16), 'tp', scatter_dimens...  68.4 us
    all_gather x1, waiting for transfers between devices, local(): lax.all_gather(lax.all_to_all(dispatch, 'sp', split_axis=0, concat_axis=0...  49.6 us
    all_to_all x1, blocking collectives, local(): lax.all_to_all(dispatch, 'sp', split_axis=0, concat_axis=0, tiled=True)  17.8 us
    dot_general x1, matrix products, local(): jnp.dot(activated, w_down[0], preferred_element_type=jnp.float32)  9.19 us
    all_to_all x1, starting transfers between devices, local(): lax.all_to_all(mixed_rows, 'tp', split_axis=0, concat_axis=1, tiled=True)  8.57 us
    all_to_all x1, waiting for transfers between devices, local(): lax.all_to_all(summed, 'sp', split_axis=0, concat_axis=0, tiled=True)  8.56 us
    all_to_all x1, waiting for transfers between devices, local(): lax.all_to_all(mixed_rows, 'tp', split_axis=0, concat_axis=1, tiled=True)  7.73 us
    all_to_all x1, starting transfers between devices, local(): lax.all_to_all(summed, 'sp', split_axis=0, concat_axis=0, tiled=True)  7.27 us
  transfers between devices with their start and end apart: 6, of which 4 were waited for; matrix products, arithmetic and copies ran while one was open for 3% of the time, Pallas kernels for 0%

commit v1 on v0

v1 whole, which is shorter than its diff:
```python
import functools

import jax
import jax.numpy as jnp
from jax import lax
from jax.experimental import pallas as pl
from jax.experimental.pallas import tpu as pltpu
from jax.sharding import Mesh, PartitionSpec as P


LANES = 128
MINOR = (((1,), (1,)), ((), ()))
VMEM = pl.BlockSpec(memory_space=pltpu.VMEM)


def call(kernel, outs, args, flops, scratch=(), limit_mib=16):
    moved = sum(a.size * a.dtype.itemsize for a in (*args, *outs))
    return pl.pallas_call(
        kernel,
        out_shape=list(outs),
        in_specs=[VMEM] * len(args),
        out_specs=[VMEM] * len(outs),
        scratch_shapes=list(scratch),
        compiler_params=pltpu.CompilerParams(vmem_limit_bytes=limit_mib * 1024 * 1024),
        cost_estimate=pl.CostEstimate(flops=flops, bytes_accessed=moved, transcendentals=0),
    )(*args)


def out(shape, dtype=jnp.bfloat16):
    return jax.ShapeDtypeStruct(shape, dtype)


def edge_kernel(gate_ref, value_ref, docs_ref, edge_ref):
    channels, length = gate_ref.shape
    tail = slice(length - LANES, length)
    edge_ref[0:channels, :] = gate_ref[:, tail]
    edge_ref[channels : 2 * channels, :] = value_ref[:, tail]
    docs = docs_ref[docs_ref.shape[0] - 1 :, :].astype(jnp.float32)
    edge_ref[2 * channels :, :] = jnp.broadcast_to(docs, (16, LANES)).astype(jnp.bfloat16)


def conv_kernel(b_ref, c_ref, v_ref, taps_ref, docs_ref, edge_ref, packed_ref):
    channels, length = b_ref.shape
    blocks, half, _ = packed_ref.shape

    def wide(ref):
        return ref.astype(jnp.float32)

    product = wide(c_ref[...]) * wide(v_ref[...])
    edge = wide(edge_ref[...])
    before = edge[0:channels] * edge[channels : 2 * channels]
    every = jnp.concatenate([before, product], axis=1)
    docs_here = jnp.concatenate(
        [wide(docs_ref[i : i + 1, :]) for i in range(docs_ref.shape[0])], axis=1
    )
    docs = jnp.concatenate([edge[2 * channels : 2 * channels + 1], docs_here], axis=1)
    docs = jnp.broadcast_to(docs, (8, docs.shape[1]))
    eye = lax.broadcasted_iota(jnp.int32, (channels, channels), 0) == lax.broadcasted_iota(
        jnp.int32, (channels, channels), 1
    )
    taps = wide(taps_ref[...])

    def tap(k):
        row = jnp.broadcast_to(taps[k : k + 1, :], (channels, channels))
        return jnp.sum(jnp.where(eye, row, 0.0), axis=1, keepdims=True)

    def back(distance):
        near = pltpu.roll(docs, distance, 1)[0:1, LANES:] == docs_here
        return pltpu.roll(every, distance, 1)[:, LANES:], near.astype(jnp.float32)

    one, near = back(1)
    two, far = back(2)
    convolved = tap(2) * product + tap(1) * one * near + tap(0) * two * far
    mixed = wide(b_ref[...]) * convolved
    pair = jnp.concatenate([mixed, pltpu.roll(mixed, length - half, 1)], axis=0).T
    packed_ref[...] = pair.reshape(blocks, 2 * half, 2 * channels)[:, :half].astype(jnp.bfloat16)


def route_kernel(capacity, ids_ref, weights_ref, place_ref, blend_ref):
    slots, tokens = place_ref.shape
    shape = (slots, tokens)
    slot = lax.broadcasted_iota(jnp.int32, shape, 0)
    expert = slot // capacity
    first = jnp.broadcast_to(ids_ref[0:1, :], shape) == expert
    second = jnp.broadcast_to(ids_ref[1:2, :], shape) == expert
    named = (first | second).astype(jnp.float32)
    earlier = lax.broadcasted_iota(jnp.int32, (tokens, tokens), 0) < lax.broadcasted_iota(
        jnp.int32, (tokens, tokens), 1
    )
    rank = jnp.dot(
        named.astype(jnp.bfloat16), earlier.astype(jnp.bfloat16), preferred_element_type=jnp.float32
    )
    here = (named > 0) & (rank.astype(jnp.int32) == slot - expert * capacity)
    place_ref[...] = here.astype(jnp.bfloat16)
    share = jnp.where(
        first,
        jnp.broadcast_to(weights_ref[0:1, :], shape),
        jnp.broadcast_to(weights_ref[1:2, :], shape),
    )
    share = jnp.where(here, share, 0.0)
    share = jnp.concatenate([share, jnp.zeros((slots, LANES - tokens), jnp.float32)], axis=1).T
    rest = share[:tokens]
    for i in range(3):
        term = rest.astype(jnp.bfloat16)
        blend_ref[:, i * slots : (i + 1) * slots] = term
        rest = rest - term.astype(jnp.float32)


def project_kernel(parts_ref, w_ref, resid_ref, gain_ref, place_ref, hidden_ref, sent_ref):
    sources, half, lanes = parts_ref.shape
    channels = lanes // 2
    left = lax.broadcasted_iota(jnp.int32, (half, lanes), 1) < channels
    early, late = [], []
    for i in range(0, sources, 2):
        a = parts_ref[i].astype(jnp.float32)
        b = parts_ref[i + 1].astype(jnp.float32)
        early.append(jnp.where(left, a, pltpu.roll(b, channels, 1)))
        late.append(jnp.where(left, pltpu.roll(a, channels, 1), b))
    rows = jnp.concatenate(
        [jnp.concatenate(early, axis=1), jnp.concatenate(late, axis=1)], axis=0
    ).astype(jnp.bfloat16)
    projected = jnp.dot(rows, w_ref[...], preferred_element_type=jnp.float32)
    hidden = (resid_ref[...].astype(jnp.float32) + projected).astype(jnp.bfloat16)
    hidden_ref[...] = hidden
    wide = hidden.astype(jnp.float32)
    scale = lax.rsqrt(jnp.mean(wide * wide, axis=-1, keepdims=True) + 1e-06)
    normed = (wide * scale * gain_ref[...].astype(jnp.float32)).astype(jnp.bfloat16)
    sent_ref[...] = jnp.dot(
        place_ref[...], normed, preferred_element_type=jnp.float32
    ).astype(jnp.bfloat16)


def combine_kernel(returned_ref, blend_ref, hidden_ref, out_ref):
    slots = returned_ref.shape[0]
    total = None
    for i in range(2, -1, -1):
        term = jnp.dot(
            blend_ref[:, i * slots : (i + 1) * slots],
            returned_ref[...],
            preferred_element_type=jnp.float32,
        )
        total = term if total is None else total + term
    out_ref[...] = (hidden_ref[...].astype(jnp.float32) + total).astype(jnp.bfloat16)


def expert_kernel(count, *refs):
    rows_in, weights = refs[:count], refs[count : count + 6]
    rows_out, (rows, activated) = refs[count + 6 : 2 * count + 6], refs[2 * count + 6 :]
    gates, ups, downs = weights[0:2], weights[2:4], weights[4:6]
    each, model = rows_in[0].shape
    for i in range(count):
        rows[i * each : (i + 1) * each, :] = rows_in[i][...]
    for half in range(2):
        gate = lax.dot_general(gates[half][...], rows[...], MINOR, preferred_element_type=jnp.float32)
        up = lax.dot_general(ups[half][...], rows[...], MINOR, preferred_element_type=jnp.float32)
        value = gate * jax.nn.sigmoid(gate) * up
        activated[half] = value.T.astype(jnp.bfloat16)
    tile = 256

    def project(n, carry):
        columns = pl.ds(pl.multiple_of(n * tile, tile), tile)
        total = jnp.dot(activated[0], downs[0][:, columns], preferred_element_type=jnp.float32)
        total = total + jnp.dot(
            activated[1], downs[1][:, columns], preferred_element_type=jnp.float32
        )
        for i in range(count):
            rows_out[i][:, columns] = total[i * each : (i + 1) * each].astype(jnp.bfloat16)
        return carry

    lax.fori_loop(0, model // tile, project, 0)


def expert(blocks, weights):
    count, (each, model) = len(blocks), blocks[0].shape
    units = weights[0].shape[0]
    return call(
        functools.partial(expert_kernel, count),
        [out((each, model))] * count,
        [*blocks, *weights],
        flops=2 * 3 * count * each * model * 2 * units,
        scratch=[
            pltpu.VMEM((count * each, model), jnp.bfloat16),
            pltpu.VMEM((2, count * each, units), jnp.bfloat16),
        ],
        limit_mib=24,
    )


def around(block, step):
    size = lax.axis_size("z")
    return lax.ppermute(block, "z", [(i, (i + step) % size) for i in range(size)])


def swapped(block):
    return lax.ppermute(block, "core", [(0, 1), (1, 0)])


def plus(a, b):
    return (a.astype(jnp.float32) + b.astype(jnp.float32)).astype(jnp.bfloat16)


UP, DOWN = 1, -1
WAYS = (UP, DOWN)
LEAD = {UP: 0, DOWN: 1}


def routed(own, weights):
    pieces = (0, 1)
    held = {(way, 0, c): own[c] for way in WAYS for c in pieces}
    sums = {}

    def serve(owners):
        sums.update(zip(owners, expert(list(owners.values()), weights)))

    def gather(step, lead):
        for way in WAYS:
            c = LEAD[way] if lead else 1 - LEAD[way]
            held[way, step, c] = around(held[way, step - 1, c], way)

    def came(step, lead):
        blocks = {}
        for way in WAYS:
            c = LEAD[way] if lead else 1 - LEAD[way]
            blocks[-way * step if step < 4 else 4, c] = held[way, step, c]
        return blocks

    gather(1, True)
    gather(1, False)
    serve({(0, c): own[c] for c in pieces})
    for step in (1, 2, 3):
        gather(step + 1, True)
        serve(came(step, True) | (came(step - 1, False) if step > 1 else {}))
        if step < 3:
            gather(step + 1, False)
    serve(came(4, True) | came(3, False))

    running = {}
    for step in (1, 2, 3, 4):
        for lead in (False, True):
            for way in WAYS:
                c = LEAD[way] if lead else 1 - LEAD[way]
                if step == 1 and not lead:
                    continue
                part = sums[4 if step == 1 else way * (5 - step), c]
                if (way, c) in running:
                    part = plus(part, running[way, c])
                running[way, c] = around(part, way)
    total = [
        sums[0, c].astype(jnp.float32)
        + running[UP, c].astype(jnp.float32)
        + running[DOWN, c].astype(jnp.float32)
        for c in pieces
    ]
    return jnp.concatenate(total, axis=0).astype(jnp.bfloat16)


def local(
    gate_b,
    gate_c,
    values_in,
    conv_w,
    documents,
    w_out,
    resid,
    norm_gain,
    route_ids,
    route_weight,
    w_gate,
    w_up,
    w_down,
):
    own_weights = [w_gate[0].T, w_up[0].T, w_down[0]]
    seq_rows, channels = gate_b.shape
    rows, model = resid.shape
    columns = lax.axis_size("sp")
    capacity = 4 * rows // columns
    slots = columns * capacity
    splits = seq_rows // rows

    docs = documents.reshape(-1, LANES)
    (edge,) = call(
        edge_kernel, [out((2 * channels + 16, LANES))], [gate_c.T, values_in.T, docs], flops=1000
    )
    before = lax.ppermute(edge, "sp", [(i, i + 1) for i in range(columns - 1)])
    place, blend = call(
        functools.partial(route_kernel, capacity),
        [out((slots, rows)), out((rows, 3 * slots))],
        [route_ids.T, route_weight.T],
        flops=10_000_000,
    )
    (packed,) = call(
        conv_kernel,
        [out((splits, rows // 2, 2 * channels))],
        [gate_b.T, gate_c.T, values_in.T, conv_w, docs, before],
        flops=10_000_000,
    )
    parts = lax.all_to_all(packed, ("z", "core"), split_axis=0, concat_axis=0, tiled=True)
    hidden, sent = call(
        project_kernel,
        [out((rows, model)), out((slots, model))],
        [parts, w_out, resid, norm_gain.reshape(1, model), place],
        flops=2_000_000_000,
    )
    others = [swapped(w) for w in own_weights]
    sent, *others = lax.optimization_barrier((sent, *others))
    weights = [w for pair in zip(own_weights, others) for w in pair]
    arrived = lax.all_to_all(
        sent.reshape(columns, capacity, model), "sp", split_axis=0, concat_axis=0, tiled=True
    ).reshape(slots, model)
    summed = routed([arrived[: slots // 2], arrived[slots // 2 :]], weights)
    returned = lax.all_to_all(
        summed.reshape(columns, capacity, model), "sp", split_axis=0, concat_axis=0, tiled=True
    ).reshape(slots, model)
    return call(
        combine_kernel, [out((rows, model))], [returned, blend, hidden], flops=50_000_000
    )[0]


def solution(mesh):
    cells = Mesh(mesh.devices.reshape(mesh.shape["sp"], -1, 2), ("sp", "z", "core"))
    tp = ("z", "core")
    every = ("sp", "z", "core")
    return jax.shard_map(
        local,
        mesh=cells,
        in_specs=(
            P("sp", tp),
            P("sp", tp),
            P("sp", tp),
            P(None, tp),
            P("sp"),
            P(),
            P(every, None),
            P(),
            P(every, None),
            P(every, None),
            P("sp", None, tp),
            P("sp", None, tp),
            P("sp", tp, None),
        ),
        out_specs=P(every, None),
        check_vma=False,
    )
```

time: 235 us -> 173 us (0.74)
  waiting for transfers between devices: 134 us -> 44.9 us
  Pallas kernels: 0 us -> 36 us
  starting transfers between devices: 22.4 us -> 49.8 us
  matrix products: 25.4 us -> 0 us
  between operations: 13.6 us -> 0.32 us
  blocking collectives: 17.8 us -> 30.9 us
  other arithmetic: 7.69 us -> 0.89 us
  local copies, waits for them, and re-layouts: 13.1 us -> 9.08 us
    reduce_scatter x1 -> x0, waiting for transfers between devices: 68.4 us -> none  [local(): lax.psum_scatter(partial_value.astype(jnp.bfloat16), 'tp', scatter_dimens...]
    all_gather x1 -> x0, waiting for transfers between devices: 49.6 us -> none  [local(): lax.all_gather(lax.all_to_all(dispatch, 'sp', split_axis=0, concat_axis=0...]
    ppermute x2 -> x32, waiting for transfers between devices: 0.01 us -> 39.4 us  [the longest x28 36.9 us: around(): lax.ppermute(block, 'z', [(i, (i + step) % size) for i in range(size)])]
    pallas_call x0 -> x10, Pallas kernels: none -> 36 us  [call(): pl.pallas_call(kernel, out_shape=list(outs), in_specs=[VMEM] * len(args),...]
    ppermute x2 -> x32, starting transfers between devices: 6.49 us -> 41.2 us  [the longest x28 37.3 us: around(): lax.ppermute(block, 'z', [(i, (i + step) % size) for i in range(size)])]
    dot_general x5 -> x0, matrix products: 25.4 us -> none  [the longest x1 9.19 us: local(): jnp.dot(activated, w_down[0], preferred_element_type=jnp.float32)]
    all_to_all x1 -> x2, blocking collectives: 17.8 us -> 30.9 us  [the longest x1 18.1 us: local(): lax.all_to_all(sent.reshape(columns, capacity, model), 'sp', split_axis=0...]
    all_to_all x2 -> x1, waiting for transfers between devices: 16.3 us -> 5.54 us  [local(): lax.all_to_all(packed, ('z', 'core'), split_axis=0, concat_axis=0, tiled=...]
  transfers between devices with their start and end apart: 6 -> 33, of which waited for: 4 -> 13; matrix products, arithmetic and copies ran while one was open for 3% -> 1% of each run, Pallas kernels for 0% -> 20%
where the time goes in v1:
time: 173 us; the launch traced here: 172 us
  starting transfers between devices  49.8 us (29%)
  waiting for transfers between devices  44.9 us (26%)
  Pallas kernels  36 us (21%)
  blocking collectives  30.9 us (18%)
  local copies, waits for them, and re-layouts  9.08 us (5%)
    ppermute x28, starting transfers between devices, around(): lax.ppermute(block, 'z', [(i, (i + step) % size) for i in range(size)])  37.3 us
    ppermute x28, waiting for transfers between devices, around(): lax.ppermute(block, 'z', [(i, (i + step) % size) for i in range(size)])  36.9 us
    pallas_call x10, Pallas kernels, call(): pl.pallas_call(kernel, out_shape=list(outs), in_specs=[VMEM] * len(args),...  36 us
    all_to_all x1, blocking collectives, local(): lax.all_to_all(sent.reshape(columns, capacity, model), 'sp', split_axis=0...  18.1 us
    all_to_all x1, blocking collectives, local(): lax.all_to_all(summed.reshape(columns, capacity, model), 'sp', split_axis...  12.7 us
    all_to_all x1, starting transfers between devices, local(): lax.all_to_all(packed, ('z', 'core'), split_axis=0, concat_axis=0, tiled=...  8.57 us
    unnamed x24, local copies, waits for them, and re-layouts  8.34 us
    all_to_all x1, waiting for transfers between devices, local(): lax.all_to_all(packed, ('z', 'core'), split_axis=0, concat_axis=0, tiled=...  5.54 us
  transfers between devices with their start and end apart: 33, of which 13 were waited for; matrix products, arithmetic and copies ran while one was open for 1% of the time, Pallas kernels for 20%

profile of v1, /device:TPU:2, one launch (start us, length us, event | category | flops | bytes accessed | tf_op | source)
XLA Modules:
  0.0 171.8 jit_solution(3763506834156210805)
XLA Ops:
  2.9 3.4 %collective-permute-start = (bf16[144,128]{1,0:T(8,128)(2,1)S(1)}, bf16[144,128]{1,0:T(8,128)(2,1)S(1)}, u32[]{:S(2)}, u32[]{:S(2)}) collective-permute-start(bf16[144,128]{1,0:T(8,128)(2,1)S(1)} %shard_map.127), channel_id=1, source_target_pairs={{0,16},{16,32},{32,48},{48,64},{64,80},{80,96},{96,112},{112,128},... | collective-permute-start | bytes 110600 | tf_op jit(solution)/shard_map/ppermute | solution.py:284
  6.3 2.4 %collective-permute-done.edge_ref = bf16[144,128]{1,0:T(8,128)(2,1)S(1)} collective-permute-done((bf16[144,128]{1,0:T(8,128)(2,1)S(1)}, bf16[144,128]{1,0:T(8,128)(2,1)S(1)}, u32[]{:S(2)}, u32[]{:S(2)}) %collective-permute-start) | collective-permute-done | bytes 36896 | tf_op jit(solution)/shard_map/ppermute | solution.py:284
  11.3 8.6 %all-to-all-start = ((bf16[16,16,128]{2,1,0:T(8,128)(2,1)}), bf16[16,16,128]{2,1,0:T(8,128)(2,1)S(1)}, u32[]{:S(2)}, u32[]{:S(2)}) async-start(bf16[16,16,128]{2,1,0:T(8,128)(2,1)} %shard_map.128), calls=%async_computation | async-start | bytes 131072 | tf_op jit(solution)/shard_map/all_to_all | solution.py:297
  22.1 5.5 %all-to-all-done.parts_ref = bf16[16,16,128]{2,1,0:T(8,128)(2,1)S(1)} async-done(((bf16[16,16,128]{2,1,0:T(8,128)(2,1)}), bf16[16,16,128]{2,1,0:T(8,128)(2,1)S(1)}, u32[]{:S(2)}, u32[]{:S(2)}) %all-to-all-start) | async-done | bytes 65568 | tf_op jit(solution)/shard_map/all_to_all | solution.py:297
  27.6 2.2 %copy-done.8 = bf16[1024,2048]{1,0:T(8,128)(2,1)S(1)} copy-done((bf16[1024,2048]{1,0:T(8,128)(2,1)S(1)}, bf16[1024,2048]{1,0:T(8,128)(2,1)}, u32[]{:S(2)}) %copy-start.8) | copy-done | bytes 4194328
  32.0 18.1 %all_to_all.15 = bf16[16,8,2048]{2,1,0:T(8,128)(2,1)S(1)} all-to-all(bf16[16,8,2048]{2,1,0:T(8,128)(2,1)S(1)} %bitcast.40), channel_id=1, replica_groups=mesh['sp'=16,'z'=8,'core'=2] {'sp'}, dimensions={0} | all-to-all | bytes 1048576 | tf_op jit(solution)/shard_map/all_to_all | solution.py:307
  50.7 1.6 collective-permute-start.4
  52.8 2.8 %collective-permute-start.9 = (bf16[64,2048]{1,0:T(8,128)(2,1)S(1)}, bf16[64,2048]{1,0:T(8,128)(2,1)S(1)}, u32[]{:S(2)}, u32[]{:S(2)}) collective-permute-start(bf16[64,2048]{1,0:T(8,128)(2,1)S(1)} %get-tuple-element.54.refs_0_), channel_id=1, source_target_pairs={{0,14},{2,0},{4,2},{6,4},{8,6},{10,8},{12,10},{14,12},{1,15},{3,1}... | collective-permute-start | bytes 786440 | tf_op jit(solution)/shard_map/ppermute | solution.py:191
  55.6 3.9 %collective-permute-done.6.refs_1_ = bf16[64,2048]{1,0:T(8,128)(2,1)S(1)} collective-permute-done((bf16[64,2048]{1,0:T(8,128)(2,1)S(1)}, bf16[64,2048]{1,0:T(8,128)(2,1)S(1)}, u32[]{:S(2)}, u32[]{:S(2)}) %collective-permute-start.6) | collective-permute-done | bytes 262176 | tf_op jit(solution)/shard_map/ppermute | solution.py:191
  61.5 5.2 %collective-permute-done.8.refs_2_ = bf16[64,2048]{1,0:T(8,128)(2,1)S(1)} collective-permute-done((bf16[64,2048]{1,0:T(8,128)(2,1)S(1)}, bf16[64,2048]{1,0:T(8,128)(2,1)S(1)}, u32[]{:S(2)}, u32[]{:S(2)}) %collective-permute-start.8) | collective-permute-done | bytes 262176 | tf_op jit(solution)/shard_map/ppermute | solution.py:191
  67.1 2.8 %collective-permute-start.13 = (bf16[64,2048]{1,0:T(8,128)(2,1)S(1)}, bf16[64,2048]{1,0:T(8,128)(2,1)S(1)}, u32[]{:S(2)}, u32[]{:S(2)}) collective-permute-start(bf16[64,2048]{1,0:T(8,128)(2,1)S(1)} %collective-permute-done.9.refs_3_), channel_id=1, source_target_pairs={{0,14},{2,0},{4,2},{6,4},{8,6},{10,8},{12,10},{14,12},{1,15},{3,1}... | collective-permute-start | bytes 786440 | tf_op jit(solution)/shard_map/ppermute | solution.py:191
  72.7 6.2 %shard_map.131 = (bf16[64,2048]{1,0:T(8,128)(2,1)S(1)}, bf16[64,2048]{1,0:T(8,128)(2,1)S(1)}) custom-call(bf16[64,2048]{1,0:T(8,128)(2,1)S(1)} %get-tuple-element.54.refs_0_, bf16[64,2048]{1,0:T(8,128)(2,1)S(1)} %get-tuple-element.53.refs_1_, bf16[448,2048]{1,0:T(8,128)(2,1)S(1)} %bitcast.22, bf16[448,2048]{1,0:T(8,128)(2,1)S(1)} %collective-permute-done.1.refs_3_.refs_5_, ...), custom_call_target="tpu_custom_call" | custom-call | flops 1409286144 | bytes 12058624 | tf_op jit(solution)/shard_map/pallas_call | solution.py:18
  78.9 6.2 %shard_map.135 = (bf16[64,2048]{1,0:T(8,128)(2,1)S(1)}, bf16[64,2048]{1,0:T(8,128)(2,1)S(1)}) custom-call(bf16[64,2048]{1,0:T(8,128)(2,1)S(1)} %collective-permute-done.4.refs_0_, bf16[64,2048]{1,0:T(8,128)(2,1)S(1)} %collective-permute-done.6.refs_1_, bf16[448,2048]{1,0:T(8,128)(2,1)S(1)} %bitcast.23, ...), custom_call_target="tpu_custom_call" | custom-call | flops 1409286144 | bytes 12058624 | tf_op jit(solution)/shard_map/pallas_call | solution.py:18
  85.7 2.8 %collective-permute-start.17 = (bf16[64,2048]{1,0:T(8,128)(2,1)S(1)}, bf16[64,2048]{1,0:T(8,128)(2,1)S(1)}, u32[]{:S(2)}, u32[]{:S(2)}) collective-permute-start(bf16[64,2048]{1,0:T(8,128)(2,1)S(1)} %collective-permute-done.13.refs_3_), channel_id=1, source_target_pairs={{0,14},{2,0},{4,2},{6,4},{8,6},{10,8},{12,10},{14,12},{1,15},{3,1}... | collective-permute-start | bytes 786440 | tf_op jit(solution)/shard_map/ppermute | solution.py:191
  88.4 6.7 %shard_map.133 = (bf16[64,2048]{1,0:T(8,128)(2,1)S(1)}, bf16[64,2048]{1,0:T(8,128)(2,1)S(1)}, bf16[64,2048]{1,0:T(8,128)(2,1)S(1)}, bf16[64,2048]{1,0:T(8,128)(2,1)S(1)}) custom-call(bf16[64,2048]{1,0:T(8,128)(2,1)S(1)} %collective-permute-done.10.refs_0_, bf16[64,2048]{1,0:T(8,128)(2,1)S(1)} %collective-permute-done.11.refs_1_, ...), custom_call_target="tpu_custom_call" | custom-call | flops 2818572288 | bytes 13107200 | tf_op jit(solution)/shard_map/pallas_call | solution.py:18
  95.2 1.7 collective-permute-start.22
  96.8 6.7 %shard_map.132 = (bf16[64,2048]{1,0:T(8,128)(2,1)S(1)}, bf16[64,2048]{1,0:T(8,128)(2,1)S(1)}, bf16[64,2048]{1,0:T(8,128)(2,1)S(1)}, bf16[64,2048]{1,0:T(8,128)(2,1)S(1)}) custom-call(bf16[64,2048]{1,0:T(8,128)(2,1)S(1)} %collective-permute-done.5.refs_0_, bf16[64,2048]{1,0:T(8,128)(2,1)S(1)} %collective-permute-done.7.refs_1_, ...), custom_call_target="tpu_custom_call" | custom-call | flops 2818572288 | bytes 13107200 | tf_op jit(solution)/shard_map/pallas_call | solution.py:18
  104.1 2.8 %collective-permute-start.15 = (bf16[64,2048]{1,0:T(8,128)(2,1)S(1)}, bf16[64,2048]{1,0:T(8,128)(2,1)S(1)}, u32[]{:S(2)}, u32[]{:S(2)}) collective-permute-start(bf16[64,2048]{1,0:T(8,128)(2,1)S(1)} %collective-permute-done.11.refs_1_), channel_id=1, source_target_pairs={{0,14},{2,0},{4,2},{6,4},{8,6},{10,8},{12,10},{14,12},{1,15},{3,1}... | collective-permute-start | bytes 786440 | tf_op jit(solution)/shard_map/ppermute | solution.py:191
  106.9 6.1 %collective-permute-done.25 = bf16[64,2048]{1,0:T(8,128)(2,1)S(1)} collective-permute-done((bf16[64,2048]{1,0:T(8,128)(2,1)S(1)}, bf16[64,2048]{1,0:T(8,128)(2,1)S(1)}, u32[]{:S(2)}, u32[]{:S(2)}) %collective-permute-start.25) | collective-permute-done | bytes 262176 | tf_op jit(solution)/shard_map/ppermute | solution.py:191
  113.1 2.3 %collective-permute-start.26 = (bf16[64,2048]{1,0:T(8,128)(2,1)S(1)}, bf16[64,2048]{1,0:T(8,128)(2,1)S(1)}, u32[]{:S(2)}, u32[]{:S(2)}) collective-permute-start(bf16[64,2048]{1,0:T(8,128)(2,1)S(1)} %add_convert_fusion.5), channel_id=1, source_target_pairs={{0,2},{2,4},{4,6},{6,8},{8,10},{10,12},{12,14},{14,0},{1,3},{3,5},... | collective-permute-start | bytes 786440 | tf_op jit(solution)/shard_map/ppermute | solution.py:191
  115.5 1.4 collective-permute-done.14.refs_0_
  116.8 6.7 %shard_map.134 = (bf16[64,2048]{1,0:T(8,128)(2,1)S(1)}, bf16[64,2048]{1,0:T(8,128)(2,1)S(1)}, bf16[64,2048]{1,0:T(8,128)(2,1)S(1)}, bf16[64,2048]{1,0:T(8,128)(2,1)S(1)}) custom-call(bf16[64,2048]{1,0:T(8,128)(2,1)S(1)} %collective-permute-done.14.refs_0_, bf16[64,2048]{1,0:T(8,128)(2,1)S(1)} %collective-permute-done.15.refs_1_, ...), custom_call_target="tpu_custom_call" | custom-call | flops 2818572288 | bytes 13107200 | tf_op jit(solution)/shard_map/pallas_call | solution.py:18
  123.7 3.2 %collective-permute-start.28 = (bf16[64,2048]{1,0:T(8,128)(2,1)S(1)}, bf16[64,2048]{1,0:T(8,128)(2,1)S(1)}, u32[]{:S(2)}, u32[]{:S(2)}) collective-permute-start(bf16[64,2048]{1,0:T(8,128)(2,1)S(1)} %get-tuple-element.50), channel_id=1, source_target_pairs={{0,14},{2,0},{4,2},{6,4},{8,6},{10,8},{12,10},{14,12},{1,15},{3,1}... | collective-permute-start | bytes 786440 | tf_op jit(solution)/shard_map/ppermute | solution.py:191
  127.1 2.1 %collective-permute-start.27 = (bf16[64,2048]{1,0:T(8,128)(2,1)S(1)}, bf16[64,2048]{1,0:T(8,128)(2,1)S(1)}, u32[]{:S(2)}, u32[]{:S(2)}) collective-permute-start(bf16[64,2048]{1,0:T(8,128)(2,1)S(1)} %add_convert_fusion.4), channel_id=1, source_target_pairs={{0,2},{2,4},{4,6},{6,8},{8,10},{10,12},{12,14},{14,0},{1,3},{3,5},... | collective-permute-start | bytes 786440 | tf_op jit(solution)/shard_map/ppermute | solution.py:191
  129.2 4.0 %collective-permute-done.18 = bf16[64,2048]{1,0:T(8,128)(2,1)S(1)} collective-permute-done((bf16[64,2048]{1,0:T(8,128)(2,1)S(1)}, bf16[64,2048]{1,0:T(8,128)(2,1)S(1)}, u32[]{:S(2)}, u32[]{:S(2)}) %collective-permute-start.18) | collective-permute-done | bytes 262176 | tf_op jit(solution)/shard_map/ppermute | solution.py:191
  133.5 3.3 %collective-permute-start.29 = (bf16[64,2048]{1,0:T(8,128)(2,1)S(1)}, bf16[64,2048]{1,0:T(8,128)(2,1)S(1)}, u32[]{:S(2)}, u32[]{:S(2)}) collective-permute-start(bf16[64,2048]{1,0:T(8,128)(2,1)S(1)} %add_convert_fusion.3), channel_id=1, source_target_pairs={{0,14},{2,0},{4,2},{6,4},{8,6},{10,8},{12,10},{14,12},{1,15},{3,1}... | collective-permute-start | bytes 786440 | tf_op jit(solution)/shard_map/ppermute | solution.py:191
  136.8 5.3 %collective-permute-done.19 = bf16[64,2048]{1,0:T(8,128)(2,1)S(1)} collective-permute-done((bf16[64,2048]{1,0:T(8,128)(2,1)S(1)}, bf16[64,2048]{1,0:T(8,128)(2,1)S(1)}, u32[]{:S(2)}, u32[]{:S(2)}) %collective-permute-start.19) | collective-permute-done | bytes 262176 | tf_op jit(solution)/shard_map/ppermute | solution.py:191
  142.3 3.3 %collective-permute-start.30 = (bf16[64,2048]{1,0:T(8,128)(2,1)S(1)}, bf16[64,2048]{1,0:T(8,128)(2,1)S(1)}, u32[]{:S(2)}, u32[]{:S(2)}) collective-permute-start(bf16[64,2048]{1,0:T(8,128)(2,1)S(1)} %add_convert_fusion.2), channel_id=1, source_target_pairs={{0,14},{2,0},{4,2},{6,4},{8,6},{10,8},{12,10},{14,12},{1,15},{3,1}... | collective-permute-start | bytes 786440 | tf_op jit(solution)/shard_map/ppermute | solution.py:191
  145.6 4.5 %collective-permute-done.20 = bf16[64,2048]{1,0:T(8,128)(2,1)S(1)} collective-permute-done((bf16[64,2048]{1,0:T(8,128)(2,1)S(1)}, bf16[64,2048]{1,0:T(8,128)(2,1)S(1)}, u32[]{:S(2)}, u32[]{:S(2)}) %collective-permute-start.20) | collective-permute-done | bytes 262176 | tf_op jit(solution)/shard_map/ppermute | solution.py:191
  150.3 3.3 %collective-permute-start.31 = (bf16[64,2048]{1,0:T(8,128)(2,1)S(1)}, bf16[64,2048]{1,0:T(8,128)(2,1)S(1)}, u32[]{:S(2)}, u32[]{:S(2)}) collective-permute-start(bf16[64,2048]{1,0:T(8,128)(2,1)S(1)} %add_convert_fusion.1), channel_id=1, source_target_pairs={{0,14},{2,0},{4,2},{6,4},{8,6},{10,8},{12,10},{14,12},{1,15},{3,1}... | collective-permute-start | bytes 786440 | tf_op jit(solution)/shard_map/ppermute | solution.py:191
  153.6 4.2 %collective-permute-done.21 = bf16[64,2048]{1,0:T(8,128)(2,1)S(1)} collective-permute-done((bf16[64,2048]{1,0:T(8,128)(2,1)S(1)}, bf16[64,2048]{1,0:T(8,128)(2,1)S(1)}, u32[]{:S(2)}, u32[]{:S(2)}) %collective-permute-start.21) | collective-permute-done | bytes 262176 | tf_op jit(solution)/shard_map/ppermute | solution.py:191
  158.1 12.7 %all_to_all.16 = bf16[16,8,2048]{2,1,0:T(8,128)(2,1)S(1)} all-to-all(bf16[16,8,2048]{2,1,0:T(8,128)(2,1)S(1)} %maximum_bitcast_fusion), channel_id=1, replica_groups=mesh['sp'=16,'z'=8,'core'=2] {'sp'}, dimensions={0} | all-to-all | bytes 1048576 | tf_op jit(solution)/shard_map/all_to_all | solution.py:311
  (85 shorter events, 19.5 us)
Async XLA Ops:
  0.0 32.0 %collective-permute-start.1 = (bf16[448,2048]{1,0:T(8,128)(2,1)}, bf16[448,2048]{1,0:T(8,128)(2,1)S(1)}, u32[]{:S(2)}, u32[]{:S(2)}) collective-permute-start(bf16[448,2048]{1,0:T(8,128)(2,1)} %bitcast.21), channel_id=1, source_target_pairs={{0,1},{1,0},{2,3},{3,2},{4,5},{5,4},{6,7},{7,6},{8,9},{9,8},{10,11... | collective-permute-start | bytes 5505032 | tf_op jit(solution)/shard_map/ppermute | solution.py:195
  0.0 32.0 %collective-permute-start.2 = (bf16[448,2048]{1,0:T(8,128)(2,1)}, bf16[448,2048]{1,0:T(8,128)(2,1)}, u32[]{:S(2)}, u32[]{:S(2)}) collective-permute-start(bf16[448,2048]{1,0:T(8,128)(2,1)} %bitcast.27), channel_id=1, source_target_pairs={{0,1},{1,0},{2,3},{3,2},{4,5},{5,4},{6,7},{7,6},{8,9},{9,8},{10,11... | collective-permute-start | bytes 5505032 | tf_op jit(solution)/shard_map/ppermute | solution.py:195
  0.5 31.5 %collective-permute-start.3 = (bf16[448,2048]{1,0:T(8,128)(2,1)}, bf16[448,2048]{1,0:T(8,128)(2,1)}, u32[]{:S(2)}, u32[]{:S(2)}) collective-permute-start(bf16[448,2048]{1,0:T(8,128)(2,1)} %bitcast.33), channel_id=1, source_target_pairs={{0,1},{1,0},{2,3},{3,2},{4,5},{5,4},{6,7},{7,6},{8,9},{9,8},{10,11... | collective-permute-start | bytes 5505032 | tf_op jit(solution)/shard_map/ppermute | solution.py:195
  11.3 16.4 %all-to-all-start = ((bf16[16,16,128]{2,1,0:T(8,128)(2,1)}), bf16[16,16,128]{2,1,0:T(8,128)(2,1)S(1)}, u32[]{:S(2)}, u32[]{:S(2)}) async-start(bf16[16,16,128]{2,1,0:T(8,128)(2,1)} %shard_map.128), calls=%async_computation | async-start | bytes 131072 | tf_op jit(solution)/shard_map/all_to_all | solution.py:297
  50.2 9.3 %collective-permute-start.6 = (bf16[64,2048]{1,0:T(8,128)(2,1)S(1)}, bf16[64,2048]{1,0:T(8,128)(2,1)S(1)}, u32[]{:S(2)}, u32[]{:S(2)}) collective-permute-start(bf16[64,2048]{1,0:T(8,128)(2,1)S(1)} %get-tuple-element.53.refs_1_), channel_id=1, source_target_pairs={{0,14},{2,0},{4,2},{6,4},{8,6},{10,8},{12,10},{14,12},{1,15},{3,1}... | collective-permute-start | bytes 786440 | tf_op jit(solution)/shard_map/ppermute | solution.py:191
  50.7 10.4 %collective-permute-start.4 = (bf16[64,2048]{1,0:T(8,128)(2,1)S(1)}, bf16[64,2048]{1,0:T(8,128)(2,1)S(1)}, u32[]{:S(2)}, u32[]{:S(2)}) collective-permute-start(bf16[64,2048]{1,0:T(8,128)(2,1)S(1)} %get-tuple-element.54.refs_0_), channel_id=1, source_target_pairs={{0,2},{2,4},{4,6},{6,8},{8,10},{10,12},{12,14},{14,0},{1,3},{3,5},... | collective-permute-start | bytes 786440 | tf_op jit(solution)/shard_map/ppermute | solution.py:191
  52.3 14.4 %collective-permute-start.8 = (bf16[64,2048]{1,0:T(8,128)(2,1)S(1)}, bf16[64,2048]{1,0:T(8,128)(2,1)S(1)}, u32[]{:S(2)}, u32[]{:S(2)}) collective-permute-start(bf16[64,2048]{1,0:T(8,128)(2,1)S(1)} %get-tuple-element.53.refs_1_), channel_id=1, source_target_pairs={{0,2},{2,4},{4,6},{6,8},{8,10},{10,12},{12,14},{14,0},{1,3},{3,5},... | collective-permute-start | bytes 786440 | tf_op jit(solution)/shard_map/ppermute | solution.py:191
  52.8 14.3 %collective-permute-start.9 = (bf16[64,2048]{1,0:T(8,128)(2,1)S(1)}, bf16[64,2048]{1,0:T(8,128)(2,1)S(1)}, u32[]{:S(2)}, u32[]{:S(2)}) collective-permute-start(bf16[64,2048]{1,0:T(8,128)(2,1)S(1)} %get-tuple-element.54.refs_0_), channel_id=1, source_target_pairs={{0,14},{2,0},{4,2},{6,4},{8,6},{10,8},{12,10},{14,12},{1,15},{3,1}... | collective-permute-start | bytes 786440 | tf_op jit(solution)/shard_map/ppermute | solution.py:191
  59.5 11.2 %collective-permute-start.7 = (bf16[64,2048]{1,0:T(8,128)(2,1)S(1)}, bf16[64,2048]{1,0:T(8,128)(2,1)S(1)}, u32[]{:S(2)}, u32[]{:S(2)}) collective-permute-start(bf16[64,2048]{1,0:T(8,128)(2,1)S(1)} %collective-permute-done.6.refs_1_), channel_id=1, source_target_pairs={{0,14},{2,0},{4,2},{6,4},{8,6},{10,8},{12,10},{14,12},{1,15},{3,1}... | collective-permute-start | bytes 786440 | tf_op jit(solution)/shard_map/ppermute | solution.py:191
  61.1 11.2 %collective-permute-start.5 = (bf16[64,2048]{1,0:T(8,128)(2,1)S(1)}, bf16[64,2048]{1,0:T(8,128)(2,1)S(1)}, u32[]{:S(2)}, u32[]{:S(2)}) collective-permute-start(bf16[64,2048]{1,0:T(8,128)(2,1)S(1)} %collective-permute-done.4.refs_0_), channel_id=1, source_target_pairs={{0,2},{2,4},{4,6},{6,8},{8,10},{10,12},{12,14},{14,0},{1,3},{3,5},... | collective-permute-start | bytes 786440 | tf_op jit(solution)/shard_map/ppermute | solution.py:191
  66.7 18.4 %collective-permute-start.12 = (bf16[64,2048]{1,0:T(8,128)(2,1)S(1)}, bf16[64,2048]{1,0:T(8,128)(2,1)S(1)}, u32[]{:S(2)}, u32[]{:S(2)}) collective-permute-start(bf16[64,2048]{1,0:T(8,128)(2,1)S(1)} %collective-permute-done.8.refs_2_), channel_id=1, source_target_pairs={{0,2},{2,4},{4,6},{6,8},{8,10},{10,12},{12,14},{14,0},{1,3},{3,5},... | collective-permute-start | bytes 786440 | tf_op jit(solution)/shard_map/ppermute | solution.py:191
  67.1 18.6 %collective-permute-start.13 = (bf16[64,2048]{1,0:T(8,128)(2,1)S(1)}, bf16[64,2048]{1,0:T(8,128)(2,1)S(1)}, u32[]{:S(2)}, u32[]{:S(2)}) collective-permute-start(bf16[64,2048]{1,0:T(8,128)(2,1)S(1)} %collective-permute-done.9.refs_3_), channel_id=1, source_target_pairs={{0,14},{2,0},{4,2},{6,4},{8,6},{10,8},{12,10},{14,12},{1,15},{3,1}... | collective-permute-start | bytes 786440 | tf_op jit(solution)/shard_map/ppermute | solution.py:191
  70.7 17.7 %collective-permute-start.11 = (bf16[64,2048]{1,0:T(8,128)(2,1)S(1)}, bf16[64,2048]{1,0:T(8,128)(2,1)S(1)}, u32[]{:S(2)}, u32[]{:S(2)}) collective-permute-start(bf16[64,2048]{1,0:T(8,128)(2,1)S(1)} %collective-permute-done.7.refs_1_), channel_id=1, source_target_pairs={{0,14},{2,0},{4,2},{6,4},{8,6},{10,8},{12,10},{14,12},{1,15},{3,1}... | collective-permute-start | bytes 786440 | tf_op jit(solution)/shard_map/ppermute | solution.py:191
  72.3 16.1 %collective-permute-start.10 = (bf16[64,2048]{1,0:T(8,128)(2,1)S(1)}, bf16[64,2048]{1,0:T(8,128)(2,1)S(1)}, u32[]{:S(2)}, u32[]{:S(2)}) collective-permute-start(bf16[64,2048]{1,0:T(8,128)(2,1)S(1)} %collective-permute-done.5.refs_0_), channel_id=1, source_target_pairs={{0,2},{2,4},{4,6},{6,8},{8,10},{10,12},{12,14},{14,0},{1,3},{3,5},... | collective-permute-start | bytes 786440 | tf_op jit(solution)/shard_map/ppermute | solution.py:191
  85.1 28.0 %collective-permute-start.16 = (bf16[64,2048]{1,0:T(8,128)(2,1)S(1)}, bf16[64,2048]{1,0:T(8,128)(2,1)S(1)}, u32[]{:S(2)}, u32[]{:S(2)}) collective-permute-start(bf16[64,2048]{1,0:T(8,128)(2,1)S(1)} %collective-permute-done.12.refs_2_), channel_id=1, source_target_pairs={{0,2},{2,4},{4,6},{6,8},{8,10},{10,12},{12,14},{14,0},{1,3},{3,5},... | collective-permute-start | bytes 786440 | tf_op jit(solution)/shard_map/ppermute | solution.py:191
  85.7 29.8 %collective-permute-start.17 = (bf16[64,2048]{1,0:T(8,128)(2,1)S(1)}, bf16[64,2048]{1,0:T(8,128)(2,1)S(1)}, u32[]{:S(2)}, u32[]{:S(2)}) collective-permute-start(bf16[64,2048]{1,0:T(8,128)(2,1)S(1)} %collective-permute-done.13.refs_3_), channel_id=1, source_target_pairs={{0,14},{2,0},{4,2},{6,4},{8,6},{10,8},{12,10},{14,12},{1,15},{3,1}... | collective-permute-start | bytes 786440 | tf_op jit(solution)/shard_map/ppermute | solution.py:191
  95.2 11.7 %collective-permute-start.22 = (bf16[64,2048]{1,0:T(8,128)(2,1)S(1)}, bf16[64,2048]{1,0:T(8,128)(2,1)S(1)}, u32[]{:S(2)}, u32[]{:S(2)}) collective-permute-start(bf16[64,2048]{1,0:T(8,128)(2,1)S(1)} %get-tuple-element.42), channel_id=1, source_target_pairs={{0,14},{2,0},{4,2},{6,4},{8,6},{10,8},{12,10},{14,12},{1,15},{3,1}... | collective-permute-start | bytes 786440 | tf_op jit(solution)/shard_map/ppermute | solution.py:191
  103.6 9.5 %collective-permute-start.25 = (bf16[64,2048]{1,0:T(8,128)(2,1)S(1)}, bf16[64,2048]{1,0:T(8,128)(2,1)S(1)}, u32[]{:S(2)}, u32[]{:S(2)}) collective-permute-start(bf16[64,2048]{1,0:T(8,128)(2,1)S(1)} %get-tuple-element.46), channel_id=1, source_target_pairs={{0,2},{2,4},{4,6},{6,8},{8,10},{10,12},{12,14},{14,0},{1,3},{3,5},... | collective-permute-start | bytes 786440 | tf_op jit(solution)/shard_map/ppermute | solution.py:191
  104.1 11.4 %collective-permute-start.15 = (bf16[64,2048]{1,0:T(8,128)(2,1)S(1)}, bf16[64,2048]{1,0:T(8,128)(2,1)S(1)}, u32[]{:S(2)}, u32[]{:S(2)}) collective-permute-start(bf16[64,2048]{1,0:T(8,128)(2,1)S(1)} %collective-permute-done.11.refs_1_), channel_id=1, source_target_pairs={{0,14},{2,0},{4,2},{6,4},{8,6},{10,8},{12,10},{14,12},{1,15},{3,1}... | collective-permute-start | bytes 786440 | tf_op jit(solution)/shard_map/ppermute | solution.py:191
  106.9 10.0 %collective-permute-start.14 = (bf16[64,2048]{1,0:T(8,128)(2,1)S(1)}, bf16[64,2048]{1,0:T(8,128)(2,1)S(1)}, u32[]{:S(2)}, u32[]{:S(2)}) collective-permute-start(bf16[64,2048]{1,0:T(8,128)(2,1)S(1)} %collective-permute-done.10.refs_0_), channel_id=1, source_target_pairs={{0,2},{2,4},{4,6},{6,8},{8,10},{10,12},{12,14},{14,0},{1,3},{3,5},... | collective-permute-start | bytes 786440 | tf_op jit(solution)/shard_map/ppermute | solution.py:191
  113.1 13.8 %collective-permute-start.23 = (bf16[64,2048]{1,0:T(8,128)(2,1)S(1)}, bf16[64,2048]{1,0:T(8,128)(2,1)S(1)}, u32[]{:S(2)}, u32[]{:S(2)}) collective-permute-start(bf16[64,2048]{1,0:T(8,128)(2,1)S(1)} %add_convert_fusion.8), channel_id=1, source_target_pairs={{0,14},{2,0},{4,2},{6,4},{8,6},{10,8},{12,10},{14,12},{1,15},{3,1}... | collective-permute-start | bytes 786440 | tf_op jit(solution)/shard_map/ppermute | solution.py:191
  113.1 13.9 %collective-permute-start.26 = (bf16[64,2048]{1,0:T(8,128)(2,1)S(1)}, bf16[64,2048]{1,0:T(8,128)(2,1)S(1)}, u32[]{:S(2)}, u32[]{:S(2)}) collective-permute-start(bf16[64,2048]{1,0:T(8,128)(2,1)S(1)} %add_convert_fusion.5), channel_id=1, source_target_pairs={{0,2},{2,4},{4,6},{6,8},{8,10},{10,12},{12,14},{14,0},{1,3},{3,5},... | collective-permute-start | bytes 786440 | tf_op jit(solution)/shard_map/ppermute | solution.py:191
  123.6 9.6 %collective-permute-start.18 = (bf16[64,2048]{1,0:T(8,128)(2,1)S(1)}, bf16[64,2048]{1,0:T(8,128)(2,1)S(1)}, u32[]{:S(2)}, u32[]{:S(2)}) collective-permute-start(bf16[64,2048]{1,0:T(8,128)(2,1)S(1)} %get-tuple-element.39), channel_id=1, source_target_pairs={{0,2},{2,4},{4,6},{6,8},{8,10},{10,12},{12,14},{14,0},{1,3},{3,5},... | collective-permute-start | bytes 786440 | tf_op jit(solution)/shard_map/ppermute | solution.py:191
  123.7 9.7 %collective-permute-start.28 = (bf16[64,2048]{1,0:T(8,128)(2,1)S(1)}, bf16[64,2048]{1,0:T(8,128)(2,1)S(1)}, u32[]{:S(2)}, u32[]{:S(2)}) collective-permute-start(bf16[64,2048]{1,0:T(8,128)(2,1)S(1)} %get-tuple-element.50), channel_id=1, source_target_pairs={{0,14},{2,0},{4,2},{6,4},{8,6},{10,8},{12,10},{14,12},{1,15},{3,1}... | collective-permute-start | bytes 786440 | tf_op jit(solution)/shard_map/ppermute | solution.py:191
  127.0 26.7 %collective-permute-start.24 = (bf16[64,2048]{1,0:T(8,128)(2,1)S(1)}, bf16[64,2048]{1,0:T(8,128)(2,1)S(1)}, u32[]{:S(2)}, u32[]{:S(2)}) collective-permute-start(bf16[64,2048]{1,0:T(8,128)(2,1)S(1)} %add_convert_fusion.7), channel_id=1, source_target_pairs={{0,14},{2,0},{4,2},{6,4},{8,6},{10,8},{12,10},{14,12},{1,15},{3,1}... | collective-permute-start | bytes 786440 | tf_op jit(solution)/shard_map/ppermute | solution.py:191
  127.1 30.8 %collective-permute-start.27 = (bf16[64,2048]{1,0:T(8,128)(2,1)S(1)}, bf16[64,2048]{1,0:T(8,128)(2,1)S(1)}, u32[]{:S(2)}, u32[]{:S(2)}) collective-permute-start(bf16[64,2048]{1,0:T(8,128)(2,1)S(1)} %add_convert_fusion.4), channel_id=1, source_target_pairs={{0,2},{2,4},{4,6},{6,8},{8,10},{10,12},{12,14},{14,0},{1,3},{3,5},... | collective-permute-start | bytes 786440 | tf_op jit(solution)/shard_map/ppermute | solution.py:191
  133.3 8.8 %collective-permute-start.19 = (bf16[64,2048]{1,0:T(8,128)(2,1)S(1)}, bf16[64,2048]{1,0:T(8,128)(2,1)S(1)}, u32[]{:S(2)}, u32[]{:S(2)}) collective-permute-start(bf16[64,2048]{1,0:T(8,128)(2,1)S(1)} %add_convert_fusion.11), channel_id=1, source_target_pairs={{0,2},{2,4},{4,6},{6,8},{8,10},{10,12},{12,14},{14,0},{1,3},{3,5},... | collective-permute-start | bytes 786440 | tf_op jit(solution)/shard_map/ppermute | solution.py:191
  133.5 8.8 %collective-permute-start.29 = (bf16[64,2048]{1,0:T(8,128)(2,1)S(1)}, bf16[64,2048]{1,0:T(8,128)(2,1)S(1)}, u32[]{:S(2)}, u32[]{:S(2)}) collective-permute-start(bf16[64,2048]{1,0:T(8,128)(2,1)S(1)} %add_convert_fusion.3), channel_id=1, source_target_pairs={{0,14},{2,0},{4,2},{6,4},{8,6},{10,8},{12,10},{14,12},{1,15},{3,1}... | collective-permute-start | bytes 786440 | tf_op jit(solution)/shard_map/ppermute | solution.py:191
  142.1 7.9 %collective-permute-start.20 = (bf16[64,2048]{1,0:T(8,128)(2,1)S(1)}, bf16[64,2048]{1,0:T(8,128)(2,1)S(1)}, u32[]{:S(2)}, u32[]{:S(2)}) collective-permute-start(bf16[64,2048]{1,0:T(8,128)(2,1)S(1)} %add_convert_fusion.10), channel_id=1, source_target_pairs={{0,2},{2,4},{4,6},{6,8},{8,10},{10,12},{12,14},{14,0},{1,3},{3,5},... | collective-permute-start | bytes 786440 | tf_op jit(solution)/shard_map/ppermute | solution.py:191
  142.3 7.9 %collective-permute-start.30 = (bf16[64,2048]{1,0:T(8,128)(2,1)S(1)}, bf16[64,2048]{1,0:T(8,128)(2,1)S(1)}, u32[]{:S(2)}, u32[]{:S(2)}) collective-permute-start(bf16[64,2048]{1,0:T(8,128)(2,1)S(1)} %add_convert_fusion.2), channel_id=1, source_target_pairs={{0,14},{2,0},{4,2},{6,4},{8,6},{10,8},{12,10},{14,12},{1,15},{3,1}... | collective-permute-start | bytes 786440 | tf_op jit(solution)/shard_map/ppermute | solution.py:191
  150.2 7.7 %collective-permute-start.21 = (bf16[64,2048]{1,0:T(8,128)(2,1)S(1)}, bf16[64,2048]{1,0:T(8,128)(2,1)S(1)}, u32[]{:S(2)}, u32[]{:S(2)}) collective-permute-start(bf16[64,2048]{1,0:T(8,128)(2,1)S(1)} %add_convert_fusion.9), channel_id=1, source_target_pairs={{0,2},{2,4},{4,6},{6,8},{8,10},{10,12},{12,14},{14,0},{1,3},{3,5},... | collective-permute-start | bytes 786440 | tf_op jit(solution)/shard_map/ppermute | solution.py:191
  150.3 7.6 %collective-permute-start.31 = (bf16[64,2048]{1,0:T(8,128)(2,1)S(1)}, bf16[64,2048]{1,0:T(8,128)(2,1)S(1)}, u32[]{:S(2)}, u32[]{:S(2)}) collective-permute-start(bf16[64,2048]{1,0:T(8,128)(2,1)S(1)} %add_convert_fusion.1), channel_id=1, source_target_pairs={{0,14},{2,0},{4,2},{6,4},{8,6},{10,8},{12,10},{14,12},{1,15},{3,1}... | collective-permute-start | bytes 786440 | tf_op jit(solution)/shard_map/ppermute | solution.py:191
  (13 other events, 138.9 us)

commit v2 on v1

--- a/solution.py
+++ b/solution.py
@@ -11,14 +11,20 @@
 LANES = 128
 MINOR = (((1,), (1,)), ((), ()))
 VMEM = pl.BlockSpec(memory_space=pltpu.VMEM)
-
-
-def call(kernel, outs, args, flops, scratch=(), limit_mib=16):
+HBM = pl.BlockSpec(memory_space=pltpu.HBM)
+
+
+def call(kernel, outs, args, flops, scratch=(), limit_mib=4, far=(), near=()):
     moved = sum(a.size * a.dtype.itemsize for a in (*args, *outs))
+    placed = {i: pltpu.HBM for i in far} | {i: pltpu.VMEM for i in near}
+    args = [
+        pltpu.with_memory_space_constraint(a, placed[i]) if i in placed else a
+        for i, a in enumerate(args)
+    ]
     return pl.pallas_call(
         kernel,
         out_shape=list(outs),
-        in_specs=[VMEM] * len(args),
+        in_specs=[HBM if i in far else VMEM for i in range(len(args))],
         out_specs=[VMEM] * len(outs),
         scratch_shapes=list(scratch),
         compiler_params=pltpu.CompilerParams(vmem_limit_bytes=limit_mib * 1024 * 1024),
@@ -30,16 +36,30 @@
     return jax.ShapeDtypeStruct(shape, dtype)
 
 
-def edge_kernel(gate_ref, value_ref, docs_ref, edge_ref):
-    channels, length = gate_ref.shape
+def staged(sources, targets, sems):
+    copies = [pltpu.make_async_copy(*pair, sems.at[i]) for i, pair in enumerate(zip(sources, targets))]
+    for copy in copies:
+        copy.start()
+    return copies
+
+
+def edge_kernel(*refs):
+    *far, docs_ref, c_ref, v_ref, b_ref, taps_ref, edge_ref, sems = refs
+    copies = staged(far, (docs_ref, c_ref, v_ref, b_ref, taps_ref), sems)
+    channels, length = c_ref.shape
     tail = slice(length - LANES, length)
-    edge_ref[0:channels, :] = gate_ref[:, tail]
-    edge_ref[channels : 2 * channels, :] = value_ref[:, tail]
+    copies[0].wait()
     docs = docs_ref[docs_ref.shape[0] - 1 :, :].astype(jnp.float32)
     edge_ref[2 * channels :, :] = jnp.broadcast_to(docs, (16, LANES)).astype(jnp.bfloat16)
-
-
-def conv_kernel(b_ref, c_ref, v_ref, taps_ref, docs_ref, edge_ref, packed_ref):
+    copies[1].wait()
+    edge_ref[0:channels, :] = c_ref[:, tail]
+    copies[2].wait()
+    edge_ref[channels : 2 * channels, :] = v_ref[:, tail]
+    copies[3].wait()
+    copies[4].wait()
+
+
+def conv_kernel(docs_ref, c_ref, v_ref, b_ref, taps_ref, edge_ref, packed_ref):
     channels, length = b_ref.shape
     blocks, half, _ = packed_ref.shape
 
@@ -76,7 +96,15 @@
     packed_ref[...] = pair.reshape(blocks, 2 * half, 2 * channels)[:, :half].astype(jnp.bfloat16)
 
 
-def route_kernel(capacity, ids_ref, weights_ref, place_ref, blend_ref):
+def route_kernel(
+    capacity, ids_far, weights_far, w_far, resid_far, place_ref, blend_ref, w_ref, resid_ref, *own
+):
+    ids_ref, weights_ref, sems = own
+    copies = staged(
+        (ids_far, weights_far, w_far, resid_far), (ids_ref, weights_ref, w_ref, resid_ref), sems
+    )
+    copies[0].wait()
+    copies[1].wait()
     slots, tokens = place_ref.shape
     shape = (slots, tokens)
     slot = lax.broadcasted_iota(jnp.int32, shape, 0)
@@ -104,6 +132,8 @@
         term = rest.astype(jnp.bfloat16)
         blend_ref[:, i * slots : (i + 1) * slots] = term
         rest = rest - term.astype(jnp.float32)
+    copies[2].wait()
+    copies[3].wait()
 
 
 def project_kernel(parts_ref, w_ref, resid_ref, gain_ref, place_ref, hidden_ref, sent_ref):
@@ -124,7 +154,8 @@
     hidden_ref[...] = hidden
     wide = hidden.astype(jnp.float32)
     scale = lax.rsqrt(jnp.mean(wide * wide, axis=-1, keepdims=True) + 1e-06)
-    normed = (wide * scale * gain_ref[...].astype(jnp.float32)).astype(jnp.bfloat16)
+    gain = jnp.concatenate([gain_ref[i : i + 1, :] for i in range(gain_ref.shape[0])], axis=1)
+    normed = (wide * scale * gain.astype(jnp.float32)).astype(jnp.bfloat16)
     sent_ref[...] = jnp.dot(
         place_ref[...], normed, preferred_element_type=jnp.float32
     ).astype(jnp.bfloat16)
@@ -182,7 +213,8 @@
             pltpu.VMEM((count * each, model), jnp.bfloat16),
             pltpu.VMEM((2, count * each, units), jnp.bfloat16),
         ],
-        limit_mib=24,
+        limit_mib=16,
+        near=range(count, count + 6),
     )
 
 
@@ -277,31 +309,46 @@
     slots = columns * capacity
     splits = seq_rows // rows
 
-    docs = documents.reshape(-1, LANES)
-    (edge,) = call(
-        edge_kernel, [out((2 * channels + 16, LANES))], [gate_c.T, values_in.T, docs], flops=1000
+    inputs = [documents.reshape(-1, LANES), gate_c.T, values_in.T, gate_b.T, conv_w]
+    *inputs, edge = call(
+        edge_kernel,
+        [*(out(x.shape, x.dtype) for x in inputs), out((2 * channels + 16, LANES))],
+        inputs,
+        flops=1000,
+        far=range(5),
+        scratch=[pltpu.SemaphoreType.DMA((5,))],
     )
     before = lax.ppermute(edge, "sp", [(i, i + 1) for i in range(columns - 1)])
-    place, blend = call(
+    others = []
+    for w in own_weights:
+        others.append(swapped(w))
+    place, blend, w_out, resid = call(
         functools.partial(route_kernel, capacity),
-        [out((slots, rows)), out((rows, 3 * slots))],
-        [route_ids.T, route_weight.T],
+        [
+            out((slots, rows)),
+            out((rows, 3 * slots)),
+            out(w_out.shape, w_out.dtype),
+            out(resid.shape, resid.dtype),
+        ],
+        [route_ids.T, route_weight.T, w_out, resid],
         flops=10_000_000,
+        far=range(4),
+        scratch=[
+            pltpu.VMEM(route_ids.T.shape, route_ids.dtype),
+            pltpu.VMEM(route_weight.T.shape, route_weight.dtype),
+            pltpu.SemaphoreType.DMA((4,)),
+        ],
     )
     (packed,) = call(
-        conv_kernel,
-        [out((splits, rows // 2, 2 * channels))],
-        [gate_b.T, gate_c.T, values_in.T, conv_w, docs, before],
-        flops=10_000_000,
+        conv_kernel, [out((splits, rows // 2, 2 * channels))], [*inputs, before], flops=10_000_000
     )
     parts = lax.all_to_all(packed, ("z", "core"), split_axis=0, concat_axis=0, tiled=True)
     hidden, sent = call(
         project_kernel,
         [out((rows, model)), out((slots, model))],
-        [parts, w_out, resid, norm_gain.reshape(1, model), place],
+        [parts, w_out, resid, norm_gain.reshape(-1, LANES), place],
         flops=2_000_000_000,
     )
-    others = [swapped(w) for w in own_weights]
     sent, *others = lax.optimization_barrier((sent, *others))
     weights = [w for pair in zip(own_weights, others) for w in pair]
     arrived = lax.all_to_all(

time: 173 us -> 169 us (0.977)
  local copies, waits for them, and re-layouts: 9.08 us -> 4.21 us
  Pallas kernels: 36 us -> 39 us
  waiting for transfers between devices: 44.9 us -> 42.9 us
    unnamed x24 -> x12, local copies, waits for them, and re-layouts: 8.34 us -> 4.17 us
    pallas_call x10, Pallas kernels: 36 us -> 39 us  [call(): pl.pallas_call(kernel, out_shape=list(outs), in_specs=[HBM if i in far el...]
    all_to_all x1, waiting for transfers between devices: 5.54 us -> 3.54 us  [local(): lax.all_to_all(packed, ('z', 'core'), split_axis=0, concat_axis=0, tiled=...]
  transfers between devices with their start and end apart: 33 -> 33, of which waited for: 13 -> 13; matrix products, arithmetic and copies ran while one was open for 1% -> 0% of each run, Pallas kernels for 20% -> 23%
where the time goes in v2:
time: 169 us; the launch traced here: 168 us
  starting transfers between devices  49.8 us (29%)
  waiting for transfers between devices  42.9 us (25%)
  Pallas kernels  39 us (23%)
  blocking collectives  30.8 us (18%)
  local copies, waits for them, and re-layouts  4.21 us (2%)
    pallas_call x10, Pallas kernels, call(): pl.pallas_call(kernel, out_shape=list(outs), in_specs=[HBM if i in far el...  39 us
    ppermute x28, starting transfers between devices, around(): lax.ppermute(block, 'z', [(i, (i + step) % size) for i in range(size)])  37.3 us
    ppermute x28, waiting for transfers between devices, around(): lax.ppermute(block, 'z', [(i, (i + step) % size) for i in range(size)])  36.9 us
    all_to_all x1, blocking collectives, local(): lax.all_to_all(sent.reshape(columns, capacity, model), 'sp', split_axis=0...  18.1 us
    all_to_all x1, blocking collectives, local(): lax.all_to_all(summed.reshape(columns, capacity, model), 'sp', split_axis...  12.7 us
    all_to_all x1, starting transfers between devices, local(): lax.all_to_all(packed, ('z', 'core'), split_axis=0, concat_axis=0, tiled=...  8.57 us
    unnamed x12, local copies, waits for them, and re-layouts  4.17 us
    all_to_all x1, waiting for transfers between devices, local(): lax.all_to_all(packed, ('z', 'core'), split_axis=0, concat_axis=0, tiled=...  3.54 us
  transfers between devices with their start and end apart: 33, of which 13 were waited for; matrix products, arithmetic and copies ran while one was open for 0% of the time, Pallas kernels for 23%

profile of v2, /device:TPU:2, one launch (start us, length us, event | category | flops | bytes accessed | tf_op | source)
XLA Modules:
  0.0 168.0 jit_solution(10531142508982448674)
XLA Ops:
  1.5 3.4 %collective-permute-start = (bf16[144,128]{1,0:T(8,128)(2,1)S(1)}, bf16[144,128]{1,0:T(8,128)(2,1)S(1)}, u32[]{:S(2)}, u32[]{:S(2)}) collective-permute-start(bf16[144,128]{1,0:T(8,128)(2,1)S(1)} %get-tuple-element.42), channel_id=1, source_target_pairs={{0,16},{16,32},{32,48},{48,64},{64,80},{80,96},{96,112},{112,128},... | collective-permute-start | bytes 110600 | tf_op jit(solution)/shard_map/ppermute | solution.py:321
  4.9 2.4 %collective-permute-done.edge_ref = bf16[144,128]{1,0:T(8,128)(2,1)S(1)} collective-permute-done((bf16[144,128]{1,0:T(8,128)(2,1)S(1)}, bf16[144,128]{1,0:T(8,128)(2,1)S(1)}, u32[]{:S(2)}, u32[]{:S(2)}) %collective-permute-start) | collective-permute-done | bytes 36896 | tf_op jit(solution)/shard_map/ppermute | solution.py:321
  8.4 8.6 %all-to-all-start = ((bf16[16,16,128]{2,1,0:T(8,128)(2,1)}), bf16[16,16,128]{2,1,0:T(8,128)(2,1)S(1)}, u32[]{:S(2)}, u32[]{:S(2)}) async-start(bf16[16,16,128]{2,1,0:T(8,128)(2,1)} %shard_map.128), calls=%async_computation | async-start | bytes 131072 | tf_op jit(solution)/shard_map/all_to_all | solution.py:345
  16.9 2.3 %shard_map.129 = (bf16[128,32]{1,0:T(8,128)(2,1)S(1)}, bf16[32,384]{1,0:T(8,128)(2,1)S(1)}, bf16[1024,2048]{1,0:T(8,128)(2,1)S(1)}, bf16[32,2048]{1,0:T(8,128)(2,1)S(1)}) custom-call(s32[2,32]{1,0:T(2,128)} %bitcast.47, f32[2,32]{1,0:T(2,128)} %bitcast.48, bf16[1024,2048]{1,0:T(8,128)(2,1)} %w_far.1, bf16[32,2048]{1,0:T(8,128)(2,1)} %resid_far.1), custom_call_target="tpu_custom_call" | custom-call | flops 10000000 | bytes 8684032 | tf_op jit(solution)/shard_map/pallas_call | solution.py:24
  19.2 2.0 %copy-done.3 = bf16[1024,2048]{1,0:T(8,128)(2,1)} copy-done((bf16[1024,2048]{1,0:T(8,128)(2,1)}, bf16[1024,2048]{1,0:T(8,128)(2,1)S(1)}, u32[]{:S(2)}) %copy-start.3) | copy-done | bytes 4194328
  21.2 3.5 %all-to-all-done.parts_ref = bf16[16,16,128]{2,1,0:T(8,128)(2,1)S(1)} async-done(((bf16[16,16,128]{2,1,0:T(8,128)(2,1)}), bf16[16,16,128]{2,1,0:T(8,128)(2,1)S(1)}, u32[]{:S(2)}, u32[]{:S(2)}) %all-to-all-start) | async-done | bytes 65568 | tf_op jit(solution)/shard_map/all_to_all | solution.py:345
  24.7 2.2 %copy-done.4 = bf16[1024,2048]{1,0:T(8,128)(2,1)S(1)} copy-done((bf16[1024,2048]{1,0:T(8,128)(2,1)S(1)}, bf16[1024,2048]{1,0:T(8,128)(2,1)}, u32[]{:S(2)}) %copy-start.4) | copy-done | bytes 4194328
  28.2 18.1 %all_to_all.15 = bf16[16,8,2048]{2,1,0:T(8,128)(2,1)S(1)} all-to-all(bf16[16,8,2048]{2,1,0:T(8,128)(2,1)S(1)} %bitcast.41), channel_id=1, replica_groups=mesh['sp'=16,'z'=8,'core'=2] {'sp'}, dimensions={0} | all-to-all | bytes 1048576 | tf_op jit(solution)/shard_map/all_to_all | solution.py:354
  49.0 2.8 %collective-permute-start.9 = (bf16[64,2048]{1,0:T(8,128)(2,1)S(1)}, bf16[64,2048]{1,0:T(8,128)(2,1)S(1)}, u32[]{:S(2)}, u32[]{:S(2)}) collective-permute-start(bf16[64,2048]{1,0:T(8,128)(2,1)S(1)} %get-tuple-element.70.refs_0_), channel_id=1, source_target_pairs={{0,14},{2,0},{4,2},{6,4},{8,6},{10,8},{12,10},{14,12},{1,15},{3,1}... | collective-permute-start | bytes 786440 | tf_op jit(solution)/shard_map/ppermute | solution.py:223
  51.7 3.9 %collective-permute-done.6.refs_1_ = bf16[64,2048]{1,0:T(8,128)(2,1)S(1)} collective-permute-done((bf16[64,2048]{1,0:T(8,128)(2,1)S(1)}, bf16[64,2048]{1,0:T(8,128)(2,1)S(1)}, u32[]{:S(2)}, u32[]{:S(2)}) %collective-permute-start.6) | collective-permute-done | bytes 262176 | tf_op jit(solution)/shard_map/ppermute | solution.py:223
  57.7 5.2 %collective-permute-done.8.refs_2_ = bf16[64,2048]{1,0:T(8,128)(2,1)S(1)} collective-permute-done((bf16[64,2048]{1,0:T(8,128)(2,1)S(1)}, bf16[64,2048]{1,0:T(8,128)(2,1)S(1)}, u32[]{:S(2)}, u32[]{:S(2)}) %collective-permute-start.8) | collective-permute-done | bytes 262176 | tf_op jit(solution)/shard_map/ppermute | solution.py:223
  63.3 2.8 %collective-permute-start.13 = (bf16[64,2048]{1,0:T(8,128)(2,1)S(1)}, bf16[64,2048]{1,0:T(8,128)(2,1)S(1)}, u32[]{:S(2)}, u32[]{:S(2)}) collective-permute-start(bf16[64,2048]{1,0:T(8,128)(2,1)S(1)} %collective-permute-done.9.refs_3_), channel_id=1, source_target_pairs={{0,14},{2,0},{4,2},{6,4},{8,6},{10,8},{12,10},{14,12},{1,15},{3,1}... | collective-permute-start | bytes 786440 | tf_op jit(solution)/shard_map/ppermute | solution.py:223
  68.9 6.2 %shard_map.131 = (bf16[64,2048]{1,0:T(8,128)(2,1)S(1)}, bf16[64,2048]{1,0:T(8,128)(2,1)S(1)}) custom-call(bf16[64,2048]{1,0:T(8,128)(2,1)S(1)} %get-tuple-element.70.refs_0_, bf16[64,2048]{1,0:T(8,128)(2,1)S(1)} %get-tuple-element.69.refs_1_, bf16[448,2048]{1,0:T(8,128)(2,1)S(1)} %bitcast.23, bf16[448,2048]{1,0:T(8,128)(2,1)S(1)} %collective-permute-done.1.refs_3_.refs_5_, ...), custom_call_target="tpu_custom_call" | custom-call | flops 1409286144 | bytes 12058624 | tf_op jit(solution)/shard_map/pallas_call | solution.py:24
  75.1 6.2 %shard_map.135 = (bf16[64,2048]{1,0:T(8,128)(2,1)S(1)}, bf16[64,2048]{1,0:T(8,128)(2,1)S(1)}) custom-call(bf16[64,2048]{1,0:T(8,128)(2,1)S(1)} %collective-permute-done.4.refs_0_, bf16[64,2048]{1,0:T(8,128)(2,1)S(1)} %collective-permute-done.6.refs_1_, bf16[448,2048]{1,0:T(8,128)(2,1)S(1)} %bitcast.24, ...), custom_call_target="tpu_custom_call" | custom-call | flops 1409286144 | bytes 12058624 | tf_op jit(solution)/shard_map/pallas_call | solution.py:24
  81.8 2.8 %collective-permute-start.17 = (bf16[64,2048]{1,0:T(8,128)(2,1)S(1)}, bf16[64,2048]{1,0:T(8,128)(2,1)S(1)}, u32[]{:S(2)}, u32[]{:S(2)}) collective-permute-start(bf16[64,2048]{1,0:T(8,128)(2,1)S(1)} %collective-permute-done.13.refs_3_), channel_id=1, source_target_pairs={{0,14},{2,0},{4,2},{6,4},{8,6},{10,8},{12,10},{14,12},{1,15},{3,1}... | collective-permute-start | bytes 786440 | tf_op jit(solution)/shard_map/ppermute | solution.py:223
  84.6 6.7 %shard_map.133 = (bf16[64,2048]{1,0:T(8,128)(2,1)S(1)}, bf16[64,2048]{1,0:T(8,128)(2,1)S(1)}, bf16[64,2048]{1,0:T(8,128)(2,1)S(1)}, bf16[64,2048]{1,0:T(8,128)(2,1)S(1)}) custom-call(bf16[64,2048]{1,0:T(8,128)(2,1)S(1)} %collective-permute-done.10.refs_0_, bf16[64,2048]{1,0:T(8,128)(2,1)S(1)} %collective-permute-done.11.refs_1_, ...), custom_call_target="tpu_custom_call" | custom-call | flops 2818572288 | bytes 13107200 | tf_op jit(solution)/shard_map/pallas_call | solution.py:24
  91.3 1.7 collective-permute-start.22
  93.0 6.7 %shard_map.132 = (bf16[64,2048]{1,0:T(8,128)(2,1)S(1)}, bf16[64,2048]{1,0:T(8,128)(2,1)S(1)}, bf16[64,2048]{1,0:T(8,128)(2,1)S(1)}, bf16[64,2048]{1,0:T(8,128)(2,1)S(1)}) custom-call(bf16[64,2048]{1,0:T(8,128)(2,1)S(1)} %collective-permute-done.5.refs_0_, bf16[64,2048]{1,0:T(8,128)(2,1)S(1)} %collective-permute-done.7.refs_1_, ...), custom_call_target="tpu_custom_call" | custom-call | flops 2818572288 | bytes 13107200 | tf_op jit(solution)/shard_map/pallas_call | solution.py:24
  100.3 2.8 %collective-permute-start.15 = (bf16[64,2048]{1,0:T(8,128)(2,1)S(1)}, bf16[64,2048]{1,0:T(8,128)(2,1)S(1)}, u32[]{:S(2)}, u32[]{:S(2)}) collective-permute-start(bf16[64,2048]{1,0:T(8,128)(2,1)S(1)} %collective-permute-done.11.refs_1_), channel_id=1, source_target_pairs={{0,14},{2,0},{4,2},{6,4},{8,6},{10,8},{12,10},{14,12},{1,15},{3,1}... | collective-permute-start | bytes 786440 | tf_op jit(solution)/shard_map/ppermute | solution.py:223
  103.1 6.1 %collective-permute-done.25 = bf16[64,2048]{1,0:T(8,128)(2,1)S(1)} collective-permute-done((bf16[64,2048]{1,0:T(8,128)(2,1)S(1)}, bf16[64,2048]{1,0:T(8,128)(2,1)S(1)}, u32[]{:S(2)}, u32[]{:S(2)}) %collective-permute-start.25) | collective-permute-done | bytes 262176 | tf_op jit(solution)/shard_map/ppermute | solution.py:223
  109.3 2.3 %collective-permute-start.26 = (bf16[64,2048]{1,0:T(8,128)(2,1)S(1)}, bf16[64,2048]{1,0:T(8,128)(2,1)S(1)}, u32[]{:S(2)}, u32[]{:S(2)}) collective-permute-start(bf16[64,2048]{1,0:T(8,128)(2,1)S(1)} %add_convert_fusion.5), channel_id=1, source_target_pairs={{0,2},{2,4},{4,6},{6,8},{8,10},{10,12},{12,14},{14,0},{1,3},{3,5},... | collective-permute-start | bytes 786440 | tf_op jit(solution)/shard_map/ppermute | solution.py:223
  113.0 6.7 %shard_map.134 = (bf16[64,2048]{1,0:T(8,128)(2,1)S(1)}, bf16[64,2048]{1,0:T(8,128)(2,1)S(1)}, bf16[64,2048]{1,0:T(8,128)(2,1)S(1)}, bf16[64,2048]{1,0:T(8,128)(2,1)S(1)}) custom-call(bf16[64,2048]{1,0:T(8,128)(2,1)S(1)} %collective-permute-done.14.refs_0_, bf16[64,2048]{1,0:T(8,128)(2,1)S(1)} %collective-permute-done.15.refs_1_, ...), custom_call_target="tpu_custom_call" | custom-call | flops 2818572288 | bytes 13107200 | tf_op jit(solution)/shard_map/pallas_call | solution.py:24
  119.8 3.2 %collective-permute-start.28 = (bf16[64,2048]{1,0:T(8,128)(2,1)S(1)}, bf16[64,2048]{1,0:T(8,128)(2,1)S(1)}, u32[]{:S(2)}, u32[]{:S(2)}) collective-permute-start(bf16[64,2048]{1,0:T(8,128)(2,1)S(1)} %get-tuple-element.66), channel_id=1, source_target_pairs={{0,14},{2,0},{4,2},{6,4},{8,6},{10,8},{12,10},{14,12},{1,15},{3,1}... | collective-permute-start | bytes 786440 | tf_op jit(solution)/shard_map/ppermute | solution.py:223
  123.3 2.1 %collective-permute-start.27 = (bf16[64,2048]{1,0:T(8,128)(2,1)S(1)}, bf16[64,2048]{1,0:T(8,128)(2,1)S(1)}, u32[]{:S(2)}, u32[]{:S(2)}) collective-permute-start(bf16[64,2048]{1,0:T(8,128)(2,1)S(1)} %add_convert_fusion.4), channel_id=1, source_target_pairs={{0,2},{2,4},{4,6},{6,8},{8,10},{10,12},{12,14},{14,0},{1,3},{3,5},... | collective-permute-start | bytes 786440 | tf_op jit(solution)/shard_map/ppermute | solution.py:223
  125.4 4.0 %collective-permute-done.18 = bf16[64,2048]{1,0:T(8,128)(2,1)S(1)} collective-permute-done((bf16[64,2048]{1,0:T(8,128)(2,1)S(1)}, bf16[64,2048]{1,0:T(8,128)(2,1)S(1)}, u32[]{:S(2)}, u32[]{:S(2)}) %collective-permute-start.18) | collective-permute-done | bytes 262176 | tf_op jit(solution)/shard_map/ppermute | solution.py:223
  129.6 3.3 %collective-permute-start.29 = (bf16[64,2048]{1,0:T(8,128)(2,1)S(1)}, bf16[64,2048]{1,0:T(8,128)(2,1)S(1)}, u32[]{:S(2)}, u32[]{:S(2)}) collective-permute-start(bf16[64,2048]{1,0:T(8,128)(2,1)S(1)} %add_convert_fusion.3), channel_id=1, source_target_pairs={{0,14},{2,0},{4,2},{6,4},{8,6},{10,8},{12,10},{14,12},{1,15},{3,1}... | collective-permute-start | bytes 786440 | tf_op jit(solution)/shard_map/ppermute | solution.py:223
  132.9 5.3 %collective-permute-done.19 = bf16[64,2048]{1,0:T(8,128)(2,1)S(1)} collective-permute-done((bf16[64,2048]{1,0:T(8,128)(2,1)S(1)}, bf16[64,2048]{1,0:T(8,128)(2,1)S(1)}, u32[]{:S(2)}, u32[]{:S(2)}) %collective-permute-start.19) | collective-permute-done | bytes 262176 | tf_op jit(solution)/shard_map/ppermute | solution.py:223
  138.5 3.3 %collective-permute-start.30 = (bf16[64,2048]{1,0:T(8,128)(2,1)S(1)}, bf16[64,2048]{1,0:T(8,128)(2,1)S(1)}, u32[]{:S(2)}, u32[]{:S(2)}) collective-permute-start(bf16[64,2048]{1,0:T(8,128)(2,1)S(1)} %add_convert_fusion.2), channel_id=1, source_target_pairs={{0,14},{2,0},{4,2},{6,4},{8,6},{10,8},{12,10},{14,12},{1,15},{3,1}... | collective-permute-start | bytes 786440 | tf_op jit(solution)/shard_map/ppermute | solution.py:223
  141.8 4.5 %collective-permute-done.20 = bf16[64,2048]{1,0:T(8,128)(2,1)S(1)} collective-permute-done((bf16[64,2048]{1,0:T(8,128)(2,1)S(1)}, bf16[64,2048]{1,0:T(8,128)(2,1)S(1)}, u32[]{:S(2)}, u32[]{:S(2)}) %collective-permute-start.20) | collective-permute-done | bytes 262176 | tf_op jit(solution)/shard_map/ppermute | solution.py:223
  146.5 3.3 %collective-permute-start.31 = (bf16[64,2048]{1,0:T(8,128)(2,1)S(1)}, bf16[64,2048]{1,0:T(8,128)(2,1)S(1)}, u32[]{:S(2)}, u32[]{:S(2)}) collective-permute-start(bf16[64,2048]{1,0:T(8,128)(2,1)S(1)} %add_convert_fusion.1), channel_id=1, source_target_pairs={{0,14},{2,0},{4,2},{6,4},{8,6},{10,8},{12,10},{14,12},{1,15},{3,1}... | collective-permute-start | bytes 786440 | tf_op jit(solution)/shard_map/ppermute | solution.py:223
  149.8 4.2 %collective-permute-done.21 = bf16[64,2048]{1,0:T(8,128)(2,1)S(1)} collective-permute-done((bf16[64,2048]{1,0:T(8,128)(2,1)S(1)}, bf16[64,2048]{1,0:T(8,128)(2,1)S(1)}, u32[]{:S(2)}, u32[]{:S(2)}) %collective-permute-start.21) | collective-permute-done | bytes 262176 | tf_op jit(solution)/shard_map/ppermute | solution.py:223
  154.3 12.7 %all_to_all.16 = bf16[16,8,2048]{2,1,0:T(8,128)(2,1)S(1)} all-to-all(bf16[16,8,2048]{2,1,0:T(8,128)(2,1)S(1)} %maximum_bitcast_fusion), channel_id=1, replica_groups=mesh['sp'=16,'z'=8,'core'=2] {'sp'}, dimensions={0} | all-to-all | bytes 1048576 | tf_op jit(solution)/shard_map/all_to_all | solution.py:358
  (72 shorter events, 16.5 us)
Async XLA Ops:
  0.0 28.2 %collective-permute-start.1 = (bf16[448,2048]{1,0:T(8,128)(2,1)}, bf16[448,2048]{1,0:T(8,128)(2,1)S(1)}, u32[]{:S(2)}, u32[]{:S(2)}) collective-permute-start(bf16[448,2048]{1,0:T(8,128)(2,1)} %bitcast.22), channel_id=1, source_target_pairs={{0,1},{1,0},{2,3},{3,2},{4,5},{5,4},{6,7},{7,6},{8,9},{9,8},{10,11... | collective-permute-start | bytes 5505032 | tf_op jit(solution)/shard_map/ppermute | solution.py:227
  0.0 28.2 %collective-permute-start.2 = (bf16[448,2048]{1,0:T(8,128)(2,1)}, bf16[448,2048]{1,0:T(8,128)(2,1)}, u32[]{:S(2)}, u32[]{:S(2)}) collective-permute-start(bf16[448,2048]{1,0:T(8,128)(2,1)} %bitcast.28), channel_id=1, source_target_pairs={{0,1},{1,0},{2,3},{3,2},{4,5},{5,4},{6,7},{7,6},{8,9},{9,8},{10,11... | collective-permute-start | bytes 5505032 | tf_op jit(solution)/shard_map/ppermute | solution.py:227
  0.5 27.7 %collective-permute-start.3 = (bf16[448,2048]{1,0:T(8,128)(2,1)}, bf16[448,2048]{1,0:T(8,128)(2,1)}, u32[]{:S(2)}, u32[]{:S(2)}) collective-permute-start(bf16[448,2048]{1,0:T(8,128)(2,1)} %bitcast.34), channel_id=1, source_target_pairs={{0,1},{1,0},{2,3},{3,2},{4,5},{5,4},{6,7},{7,6},{8,9},{9,8},{10,11... | collective-permute-start | bytes 5505032 | tf_op jit(solution)/shard_map/ppermute | solution.py:227
  8.4 16.4 %all-to-all-start = ((bf16[16,16,128]{2,1,0:T(8,128)(2,1)}), bf16[16,16,128]{2,1,0:T(8,128)(2,1)S(1)}, u32[]{:S(2)}, u32[]{:S(2)}) async-start(bf16[16,16,128]{2,1,0:T(8,128)(2,1)} %shard_map.128), calls=%async_computation | async-start | bytes 131072 | tf_op jit(solution)/shard_map/all_to_all | solution.py:345
  46.4 9.3 %collective-permute-start.6 = (bf16[64,2048]{1,0:T(8,128)(2,1)S(1)}, bf16[64,2048]{1,0:T(8,128)(2,1)S(1)}, u32[]{:S(2)}, u32[]{:S(2)}) collective-permute-start(bf16[64,2048]{1,0:T(8,128)(2,1)S(1)} %get-tuple-element.69.refs_1_), channel_id=1, source_target_pairs={{0,14},{2,0},{4,2},{6,4},{8,6},{10,8},{12,10},{14,12},{1,15},{3,1}... | collective-permute-start | bytes 786440 | tf_op jit(solution)/shard_map/ppermute | solution.py:223
  46.9 10.4 %collective-permute-start.4 = (bf16[64,2048]{1,0:T(8,128)(2,1)S(1)}, bf16[64,2048]{1,0:T(8,128)(2,1)S(1)}, u32[]{:S(2)}, u32[]{:S(2)}) collective-permute-start(bf16[64,2048]{1,0:T(8,128)(2,1)S(1)} %get-tuple-element.70.refs_0_), channel_id=1, source_target_pairs={{0,2},{2,4},{4,6},{6,8},{8,10},{10,12},{12,14},{14,0},{1,3},{3,5},... | collective-permute-start | bytes 786440 | tf_op jit(solution)/shard_map/ppermute | solution.py:223
  48.5 14.4 %collective-permute-start.8 = (bf16[64,2048]{1,0:T(8,128)(2,1)S(1)}, bf16[64,2048]{1,0:T(8,128)(2,1)S(1)}, u32[]{:S(2)}, u32[]{:S(2)}) collective-permute-start(bf16[64,2048]{1,0:T(8,128)(2,1)S(1)} %get-tuple-element.69.refs_1_), channel_id=1, source_target_pairs={{0,2},{2,4},{4,6},{6,8},{8,10},{10,12},{12,14},{14,0},{1,3},{3,5},... | collective-permute-start | bytes 786440 | tf_op jit(solution)/shard_map/ppermute | solution.py:223
  49.0 14.3 %collective-permute-start.9 = (bf16[64,2048]{1,0:T(8,128)(2,1)S(1)}, bf16[64,2048]{1,0:T(8,128)(2,1)S(1)}, u32[]{:S(2)}, u32[]{:S(2)}) collective-permute-start(bf16[64,2048]{1,0:T(8,128)(2,1)S(1)} %get-tuple-element.70.refs_0_), channel_id=1, source_target_pairs={{0,14},{2,0},{4,2},{6,4},{8,6},{10,8},{12,10},{14,12},{1,15},{3,1}... | collective-permute-start | bytes 786440 | tf_op jit(solution)/shard_map/ppermute | solution.py:223
  55.7 11.2 %collective-permute-start.7 = (bf16[64,2048]{1,0:T(8,128)(2,1)S(1)}, bf16[64,2048]{1,0:T(8,128)(2,1)S(1)}, u32[]{:S(2)}, u32[]{:S(2)}) collective-permute-start(bf16[64,2048]{1,0:T(8,128)(2,1)S(1)} %collective-permute-done.6.refs_1_), channel_id=1, source_target_pairs={{0,14},{2,0},{4,2},{6,4},{8,6},{10,8},{12,10},{14,12},{1,15},{3,1}... | collective-permute-start | bytes 786440 | tf_op jit(solution)/shard_map/ppermute | solution.py:223
  57.2 11.2 %collective-permute-start.5 = (bf16[64,2048]{1,0:T(8,128)(2,1)S(1)}, bf16[64,2048]{1,0:T(8,128)(2,1)S(1)}, u32[]{:S(2)}, u32[]{:S(2)}) collective-permute-start(bf16[64,2048]{1,0:T(8,128)(2,1)S(1)} %collective-permute-done.4.refs_0_), channel_id=1, source_target_pairs={{0,2},{2,4},{4,6},{6,8},{8,10},{10,12},{12,14},{14,0},{1,3},{3,5},... | collective-permute-start | bytes 786440 | tf_op jit(solution)/shard_map/ppermute | solution.py:223
  62.9 18.4 %collective-permute-start.12 = (bf16[64,2048]{1,0:T(8,128)(2,1)S(1)}, bf16[64,2048]{1,0:T(8,128)(2,1)S(1)}, u32[]{:S(2)}, u32[]{:S(2)}) collective-permute-start(bf16[64,2048]{1,0:T(8,128)(2,1)S(1)} %collective-permute-done.8.refs_2_), channel_id=1, source_target_pairs={{0,2},{2,4},{4,6},{6,8},{8,10},{10,12},{12,14},{14,0},{1,3},{3,5},... | collective-permute-start | bytes 786440 | tf_op jit(solution)/shard_map/ppermute | solution.py:223
  63.3 18.5 %collective-permute-start.13 = (bf16[64,2048]{1,0:T(8,128)(2,1)S(1)}, bf16[64,2048]{1,0:T(8,128)(2,1)S(1)}, u32[]{:S(2)}, u32[]{:S(2)}) collective-permute-start(bf16[64,2048]{1,0:T(8,128)(2,1)S(1)} %collective-permute-done.9.refs_3_), channel_id=1, source_target_pairs={{0,14},{2,0},{4,2},{6,4},{8,6},{10,8},{12,10},{14,12},{1,15},{3,1}... | collective-permute-start | bytes 786440 | tf_op jit(solution)/shard_map/ppermute | solution.py:223
  66.9 17.7 %collective-permute-start.11 = (bf16[64,2048]{1,0:T(8,128)(2,1)S(1)}, bf16[64,2048]{1,0:T(8,128)(2,1)S(1)}, u32[]{:S(2)}, u32[]{:S(2)}) collective-permute-start(bf16[64,2048]{1,0:T(8,128)(2,1)S(1)} %collective-permute-done.7.refs_1_), channel_id=1, source_target_pairs={{0,14},{2,0},{4,2},{6,4},{8,6},{10,8},{12,10},{14,12},{1,15},{3,1}... | collective-permute-start | bytes 786440 | tf_op jit(solution)/shard_map/ppermute | solution.py:223
  68.5 16.1 %collective-permute-start.10 = (bf16[64,2048]{1,0:T(8,128)(2,1)S(1)}, bf16[64,2048]{1,0:T(8,128)(2,1)S(1)}, u32[]{:S(2)}, u32[]{:S(2)}) collective-permute-start(bf16[64,2048]{1,0:T(8,128)(2,1)S(1)} %collective-permute-done.5.refs_0_), channel_id=1, source_target_pairs={{0,2},{2,4},{4,6},{6,8},{8,10},{10,12},{12,14},{14,0},{1,3},{3,5},... | collective-permute-start | bytes 786440 | tf_op jit(solution)/shard_map/ppermute | solution.py:223
  81.3 28.0 %collective-permute-start.16 = (bf16[64,2048]{1,0:T(8,128)(2,1)S(1)}, bf16[64,2048]{1,0:T(8,128)(2,1)S(1)}, u32[]{:S(2)}, u32[]{:S(2)}) collective-permute-start(bf16[64,2048]{1,0:T(8,128)(2,1)S(1)} %collective-permute-done.12.refs_2_), channel_id=1, source_target_pairs={{0,2},{2,4},{4,6},{6,8},{8,10},{10,12},{12,14},{14,0},{1,3},{3,5},... | collective-permute-start | bytes 786440 | tf_op jit(solution)/shard_map/ppermute | solution.py:223
  81.8 29.8 %collective-permute-start.17 = (bf16[64,2048]{1,0:T(8,128)(2,1)S(1)}, bf16[64,2048]{1,0:T(8,128)(2,1)S(1)}, u32[]{:S(2)}, u32[]{:S(2)}) collective-permute-start(bf16[64,2048]{1,0:T(8,128)(2,1)S(1)} %collective-permute-done.13.refs_3_), channel_id=1, source_target_pairs={{0,14},{2,0},{4,2},{6,4},{8,6},{10,8},{12,10},{14,12},{1,15},{3,1}... | collective-permute-start | bytes 786440 | tf_op jit(solution)/shard_map/ppermute | solution.py:223
  91.3 11.7 %collective-permute-start.22 = (bf16[64,2048]{1,0:T(8,128)(2,1)S(1)}, bf16[64,2048]{1,0:T(8,128)(2,1)S(1)}, u32[]{:S(2)}, u32[]{:S(2)}) collective-permute-start(bf16[64,2048]{1,0:T(8,128)(2,1)S(1)} %get-tuple-element.58), channel_id=1, source_target_pairs={{0,14},{2,0},{4,2},{6,4},{8,6},{10,8},{12,10},{14,12},{1,15},{3,1}... | collective-permute-start | bytes 786440 | tf_op jit(solution)/shard_map/ppermute | solution.py:223
  99.7 9.5 %collective-permute-start.25 = (bf16[64,2048]{1,0:T(8,128)(2,1)S(1)}, bf16[64,2048]{1,0:T(8,128)(2,1)S(1)}, u32[]{:S(2)}, u32[]{:S(2)}) collective-permute-start(bf16[64,2048]{1,0:T(8,128)(2,1)S(1)} %get-tuple-element.62), channel_id=1, source_target_pairs={{0,2},{2,4},{4,6},{6,8},{8,10},{10,12},{12,14},{14,0},{1,3},{3,5},... | collective-permute-start | bytes 786440 | tf_op jit(solution)/shard_map/ppermute | solution.py:223
  100.3 11.4 %collective-permute-start.15 = (bf16[64,2048]{1,0:T(8,128)(2,1)S(1)}, bf16[64,2048]{1,0:T(8,128)(2,1)S(1)}, u32[]{:S(2)}, u32[]{:S(2)}) collective-permute-start(bf16[64,2048]{1,0:T(8,128)(2,1)S(1)} %collective-permute-done.11.refs_1_), channel_id=1, source_target_pairs={{0,14},{2,0},{4,2},{6,4},{8,6},{10,8},{12,10},{14,12},{1,15},{3,1}... | collective-permute-start | bytes 786440 | tf_op jit(solution)/shard_map/ppermute | solution.py:223
  103.1 10.0 %collective-permute-start.14 = (bf16[64,2048]{1,0:T(8,128)(2,1)S(1)}, bf16[64,2048]{1,0:T(8,128)(2,1)S(1)}, u32[]{:S(2)}, u32[]{:S(2)}) collective-permute-start(bf16[64,2048]{1,0:T(8,128)(2,1)S(1)} %collective-permute-done.10.refs_0_), channel_id=1, source_target_pairs={{0,2},{2,4},{4,6},{6,8},{8,10},{10,12},{12,14},{14,0},{1,3},{3,5},... | collective-permute-start | bytes 786440 | tf_op jit(solution)/shard_map/ppermute | solution.py:223
  109.2 13.8 %collective-permute-start.23 = (bf16[64,2048]{1,0:T(8,128)(2,1)S(1)}, bf16[64,2048]{1,0:T(8,128)(2,1)S(1)}, u32[]{:S(2)}, u32[]{:S(2)}) collective-permute-start(bf16[64,2048]{1,0:T(8,128)(2,1)S(1)} %add_convert_fusion.8), channel_id=1, source_target_pairs={{0,14},{2,0},{4,2},{6,4},{8,6},{10,8},{12,10},{14,12},{1,15},{3,1}... | collective-permute-start | bytes 786440 | tf_op jit(solution)/shard_map/ppermute | solution.py:223
  109.3 13.9 %collective-permute-start.26 = (bf16[64,2048]{1,0:T(8,128)(2,1)S(1)}, bf16[64,2048]{1,0:T(8,128)(2,1)S(1)}, u32[]{:S(2)}, u32[]{:S(2)}) collective-permute-start(bf16[64,2048]{1,0:T(8,128)(2,1)S(1)} %add_convert_fusion.5), channel_id=1, source_target_pairs={{0,2},{2,4},{4,6},{6,8},{8,10},{10,12},{12,14},{14,0},{1,3},{3,5},... | collective-permute-start | bytes 786440 | tf_op jit(solution)/shard_map/ppermute | solution.py:223
  119.8 9.6 %collective-permute-start.18 = (bf16[64,2048]{1,0:T(8,128)(2,1)S(1)}, bf16[64,2048]{1,0:T(8,128)(2,1)S(1)}, u32[]{:S(2)}, u32[]{:S(2)}) collective-permute-start(bf16[64,2048]{1,0:T(8,128)(2,1)S(1)} %get-tuple-element.55), channel_id=1, source_target_pairs={{0,2},{2,4},{4,6},{6,8},{8,10},{10,12},{12,14},{14,0},{1,3},{3,5},... | collective-permute-start | bytes 786440 | tf_op jit(solution)/shard_map/ppermute | solution.py:223
  119.8 9.7 %collective-permute-start.28 = (bf16[64,2048]{1,0:T(8,128)(2,1)S(1)}, bf16[64,2048]{1,0:T(8,128)(2,1)S(1)}, u32[]{:S(2)}, u32[]{:S(2)}) collective-permute-start(bf16[64,2048]{1,0:T(8,128)(2,1)S(1)} %get-tuple-element.66), channel_id=1, source_target_pairs={{0,14},{2,0},{4,2},{6,4},{8,6},{10,8},{12,10},{14,12},{1,15},{3,1}... | collective-permute-start | bytes 786440 | tf_op jit(solution)/shard_map/ppermute | solution.py:223
  123.1 26.7 %collective-permute-start.24 = (bf16[64,2048]{1,0:T(8,128)(2,1)S(1)}, bf16[64,2048]{1,0:T(8,128)(2,1)S(1)}, u32[]{:S(2)}, u32[]{:S(2)}) collective-permute-start(bf16[64,2048]{1,0:T(8,128)(2,1)S(1)} %add_convert_fusion.7), channel_id=1, source_target_pairs={{0,14},{2,0},{4,2},{6,4},{8,6},{10,8},{12,10},{14,12},{1,15},{3,1}... | collective-permute-start | bytes 786440 | tf_op jit(solution)/shard_map/ppermute | solution.py:223
  123.3 30.8 %collective-permute-start.27 = (bf16[64,2048]{1,0:T(8,128)(2,1)S(1)}, bf16[64,2048]{1,0:T(8,128)(2,1)S(1)}, u32[]{:S(2)}, u32[]{:S(2)}) collective-permute-start(bf16[64,2048]{1,0:T(8,128)(2,1)S(1)} %add_convert_fusion.4), channel_id=1, source_target_pairs={{0,2},{2,4},{4,6},{6,8},{8,10},{10,12},{12,14},{14,0},{1,3},{3,5},... | collective-permute-start | bytes 786440 | tf_op jit(solution)/shard_map/ppermute | solution.py:223
  129.5 8.8 %collective-permute-start.19 = (bf16[64,2048]{1,0:T(8,128)(2,1)S(1)}, bf16[64,2048]{1,0:T(8,128)(2,1)S(1)}, u32[]{:S(2)}, u32[]{:S(2)}) collective-permute-start(bf16[64,2048]{1,0:T(8,128)(2,1)S(1)} %add_convert_fusion.11), channel_id=1, source_target_pairs={{0,2},{2,4},{4,6},{6,8},{8,10},{10,12},{12,14},{14,0},{1,3},{3,5},... | collective-permute-start | bytes 786440 | tf_op jit(solution)/shard_map/ppermute | solution.py:223
  129.6 8.8 %collective-permute-start.29 = (bf16[64,2048]{1,0:T(8,128)(2,1)S(1)}, bf16[64,2048]{1,0:T(8,128)(2,1)S(1)}, u32[]{:S(2)}, u32[]{:S(2)}) collective-permute-start(bf16[64,2048]{1,0:T(8,128)(2,1)S(1)} %add_convert_fusion.3), channel_id=1, source_target_pairs={{0,14},{2,0},{4,2},{6,4},{8,6},{10,8},{12,10},{14,12},{1,15},{3,1}... | collective-permute-start | bytes 786440 | tf_op jit(solution)/shard_map/ppermute | solution.py:223
  138.3 7.9 %collective-permute-start.20 = (bf16[64,2048]{1,0:T(8,128)(2,1)S(1)}, bf16[64,2048]{1,0:T(8,128)(2,1)S(1)}, u32[]{:S(2)}, u32[]{:S(2)}) collective-permute-start(bf16[64,2048]{1,0:T(8,128)(2,1)S(1)} %add_convert_fusion.10), channel_id=1, source_target_pairs={{0,2},{2,4},{4,6},{6,8},{8,10},{10,12},{12,14},{14,0},{1,3},{3,5},... | collective-permute-start | bytes 786440 | tf_op jit(solution)/shard_map/ppermute | solution.py:223
  138.5 7.9 %collective-permute-start.30 = (bf16[64,2048]{1,0:T(8,128)(2,1)S(1)}, bf16[64,2048]{1,0:T(8,128)(2,1)S(1)}, u32[]{:S(2)}, u32[]{:S(2)}) collective-permute-start(bf16[64,2048]{1,0:T(8,128)(2,1)S(1)} %add_convert_fusion.2), channel_id=1, source_target_pairs={{0,14},{2,0},{4,2},{6,4},{8,6},{10,8},{12,10},{14,12},{1,15},{3,1}... | collective-permute-start | bytes 786440 | tf_op jit(solution)/shard_map/ppermute | solution.py:223
  146.3 7.7 %collective-permute-start.21 = (bf16[64,2048]{1,0:T(8,128)(2,1)S(1)}, bf16[64,2048]{1,0:T(8,128)(2,1)S(1)}, u32[]{:S(2)}, u32[]{:S(2)}) collective-permute-start(bf16[64,2048]{1,0:T(8,128)(2,1)S(1)} %add_convert_fusion.9), channel_id=1, source_target_pairs={{0,2},{2,4},{4,6},{6,8},{8,10},{10,12},{12,14},{14,0},{1,3},{3,5},... | collective-permute-start | bytes 786440 | tf_op jit(solution)/shard_map/ppermute | solution.py:223
  146.5 7.6 %collective-permute-start.31 = (bf16[64,2048]{1,0:T(8,128)(2,1)S(1)}, bf16[64,2048]{1,0:T(8,128)(2,1)S(1)}, u32[]{:S(2)}, u32[]{:S(2)}) collective-permute-start(bf16[64,2048]{1,0:T(8,128)(2,1)S(1)} %add_convert_fusion.1), channel_id=1, source_target_pairs={{0,14},{2,0},{4,2},{6,4},{8,6},{10,8},{12,10},{14,12},{1,15},{3,1}... | collective-permute-start | bytes 786440 | tf_op jit(solution)/shard_map/ppermute | solution.py:223
  (7 other events, 142.6 us)
